TPU v7x, 512 devices: a 4x2x32 block of a 4x8x32 slice. The times are simulated.
512 devices in a mesh: grp: 2 (over y), sp: 32 (over z), dp: 8 (over x, core).
Axes of the slice: x: 4, y: 2, z: 32, core: 2. Of those that a mesh axis runs over, the one named last changes fastest.
The devices are a block of a 4x8x32 slice.
Arguments:
- tokens: bfloat16 [16, 12288, 2048], P(('grp', 'dp'), 'sp'), parts along dimension 0, may hold values from -6 to 6
- w_value: bfloat16 [2048, 1024], P('dp', 'sp'), may hold values from -0.125 to 0.125
- w_gate: bfloat16 [2048, 1024], P('dp', 'sp'), may hold values from -0.125 to 0.125
- conv_weight: bfloat16 [31, 1024], replicated, may hold values from -20 to 20
- norm_gain: float32 [1024], replicated, may hold values from 0.1 to 1.9
- norm_bias: float32 [1024], replicated, may hold values from -3 to 3
- w_out: bfloat16 [1024, 2048], P('sp', 'dp'), may hold values from -0.1875 to 0.1875
Outputs:
- mixed: bfloat16 [16, 12288, 2048], P(('grp', 'dp'), 'sp'), parts along dimension 0
There are 2 independent parts, one for each index of `grp`. A program takes and returns all parts, laid end to end along the dimension named above; an argument that names none is the same for every part. Nothing has to cross between parts.
All inputs are finite; a program needn't handle non-finite values.
Results may differ from a plain program's by a relative error of at most 0.012.
Values may be sent and summed in bfloat16 or wider, within the bound.
No kernel may reach another device: no remote copies, remote signals or barrier semaphores. Data moves between devices by JAX's collectives and lax.ppermute only.
A program may use at most 64 MiB of HBM per device.

v0:
```python
import jax
import jax.numpy as jnp
from jax import lax
from jax.experimental import pallas as pl
from jax.experimental.pallas import tpu as pltpu
from jax.sharding import Mesh, PartitionSpec as P


EPS = 1e-05
HALO = 32
LANES = 128
QUARTERS = ((0, 0), (1, 0), (0, 1), (1, 1))


def copies(block, axis):
    return jnp.broadcast_to(block, (lax.axis_size(axis), *block.shape))


def exchanged(blocks, axis):
    return lax.all_to_all(blocks, axis, 0, 0)


def swapped(array, axis):
    return lax.ppermute(array, axis, [(0, 1), (1, 0)])


def columns(where_ref, x, m, deep):
    core = where_ref[0]
    c = core if m == 0 else 1 - core
    return pl.ds(pl.multiple_of((2 * x + c) * deep, deep), deep)


def chosen(array, where_ref, quarter, precision=None):
    side = where_ref[1] if quarter[0] == 0 else 1 - where_ref[1]
    parity = where_ref[2] if quarter[1] == 0 else 1 - where_ref[2]
    width = LANES // 8
    wide = 4 * LANES
    source = lax.broadcasted_iota(jnp.int32, (wide, LANES), 0)
    target = lax.broadcasted_iota(jnp.int32, (wide, LANES), 1)
    pick = source == (target // width) * (4 * width) + parity * (2 * width) + side * width + target % width
    pick = jnp.where(pick, 1.0, 0.0).astype(array.dtype)
    parts = [array[:, at : at + wide] for at in range(0, array.shape[1], wide)]
    parts = [jnp.dot(p, pick, preferred_element_type=jnp.float32, precision=precision) for p in parts]
    return jnp.concatenate(parts, axis=1)


def convolve(fresh, tok, cw, value, gate, conv_ref, stats_ref, shifted):
    rows, part = conv_ref.shape[0], value.shape[0]
    taps = cw.shape[1]
    nt = (((1,), (1,)), ((), ()))
    value = lax.dot_general(tok[...], value, nt, preferred_element_type=jnp.float32)
    gate = lax.dot_general(tok[...], gate, nt, preferred_element_type=jnp.float32)
    glu = (value * jax.nn.sigmoid(gate)).astype(jnp.bfloat16).astype(jnp.float32)
    shifted[0] = glu
    for r in range(1, 8):
        shifted[r] = pltpu.roll(glu, r, 0)
    half = rows // 2
    for at in range(0, part, LANES):
        here = slice(at, at + LANES)
        for h in range(2):
            acc = jnp.zeros((half, LANES), jnp.float32)
            for k in range(taps):
                r, j = k % 8, k // 8
                begin = HALO - 8 * j + h * half
                acc = acc + cw[0, k : k + 1, here] * shifted[r, begin : begin + half, here]
            acc = acc.astype(jnp.bfloat16)
            when = slice(h * half, (h + 1) * half)
            conv_ref[when, here] = acc
            acc = acc.astype(jnp.float32)
            if fresh and at == 0:
                stats_ref[0, when] = acc
                stats_ref[1, when] = acc * acc
            else:
                stats_ref[0, when] += acc
                stats_ref[1, when] += acc * acc


def joined(w, blocks, *index):
    return jnp.concatenate([w[(m, x, *index)] for x in range(blocks) for m in range(2)], axis=1)


def first(where_ref, halo_ref, tok_ref, cw_ref, w0_ref, w1_ref, conv_ref, stats_ref, tok_out, cw_out, tok, cw, w, shifted, taps, sems):
    blocks = w.shape[1]
    rows, deep = tok_ref.shape[0], tok.shape[1] // (2 * blocks)
    loads = [pltpu.make_async_copy(cw_ref, taps, sems.at[0])]
    for at in range(2 * blocks):
        here, there = pl.ds(at * deep, deep), columns(where_ref, at // 2, at % 2, deep)
        loads.append(pltpu.make_async_copy(halo_ref.at[:, there], tok.at[pl.ds(0, HALO), here], sems.at[5 + 2 * at]))
        loads.append(pltpu.make_async_copy(tok_ref.at[:, there], tok.at[pl.ds(HALO, rows), here], sems.at[6 + 2 * at]))
    for m, r in enumerate((w0_ref, w1_ref)):
        loads.append(pltpu.make_async_copy(r.at[:, pl.ds(0, 2)], w.at[m], sems.at[1 + m]))
    for load in loads:
        load.start()
    loads[0].wait()
    for i, quarter in enumerate(QUARTERS):
        cw[i] = chosen(taps[...], where_ref, quarter)
    for load in loads[1:]:
        load.wait()
    stores = [pltpu.make_async_copy(tok, tok_out, sems.at[3]), pltpu.make_async_copy(cw, cw_out, sems.at[4])]
    for store in stores:
        store.start()
    convolve(True, tok, cw.at[pl.ds(0, 1)], joined(w, blocks, 0), joined(w, blocks, 1), conv_ref, stats_ref, shifted)
    for store in stores:
        store.wait()


def remaining(where_ref, tok_ref, cw_ref, w0_ref, w1_ref, first_ref, stats_ref, gain_ref, bias_ref, *refs):
    o_refs, (out_ref, tok, cw, w, shifted, conv, whole, stats, more, affine, o, sems) = refs[:-12], refs[-12:]
    count, blocks, part, deep = w.shape[0], w.shape[2], w.shape[4], w.shape[5]
    channels = whole.shape[1]
    serial = iter(range(64))

    def load(source, target):
        copy = pltpu.make_async_copy(source, target, sems.at[next(serial)])
        copy.start()
        return copy

    early = [load(tok_ref, tok), load(cw_ref, cw)]
    pieces = [[load(r.at[:, i], w.at[i, m]) for m, r in enumerate((w0_ref, w1_ref))] for i in range(count)]
    middle = [load(first_ref, conv.at[0]), load(stats_ref, stats)]
    middle += [load(gain_ref, affine.at[pl.ds(0, 1)]), load(bias_ref, affine.at[pl.ds(8, 1)])]
    late = []
    for i, r in enumerate(o_refs):
        m, q = i // len(QUARTERS), i % len(QUARTERS)
        late.append(load(r.at[:, 2] if q == 0 else r, o.at[m, q]))
    for copy in early:
        copy.wait()
    for i in range(count):
        for copy in pieces[i]:
            copy.wait()
        piece = w.at[i]
        value, gate = joined(piece, blocks, 0), joined(piece, blocks, 1)
        convolve(i == 0, tok, cw.at[pl.ds(1 + i, 1)], value, gate, conv.at[1 + i], more, shifted)
    for copy in middle:
        copy.wait()
    mean = jnp.sum(stats[0] + more[0], axis=1, keepdims=True) / channels
    meansq = jnp.sum(stats[1] + more[1], axis=1, keepdims=True) / channels
    scale = lax.rsqrt(meansq - mean * mean + EPS)
    for q, quarter in enumerate(QUARTERS):
        gain, bias = (
            chosen(jnp.broadcast_to(affine[at : at + 1], (8, channels)), where_ref, quarter, lax.Precision.HIGHEST)[:1]
            for at in (0, 8)
        )
        v = (conv[q].astype(jnp.float32) - mean) * scale * gain + bias
        whole[:, q * part : (q + 1) * part] = (v / (1.0 + jnp.exp(-v))).astype(jnp.bfloat16)
    for copy in late:
        copy.wait()
    for x in range(blocks):
        for m in range(2):
            right = jnp.concatenate([o[m, q, x] for q in range(len(QUARTERS))], axis=0)
            out = jnp.dot(whole[...], right, preferred_element_type=jnp.float32)
            out_ref[:, columns(where_ref, x, m, deep)] = out.astype(jnp.bfloat16)


SMEM, VMEM, HBM, ANY = (pl.BlockSpec(memory_space=space) for space in (pltpu.SMEM, pltpu.VMEM, pltpu.HBM, pl.ANY))


def kernel(function, specs, outs, scratch, flops, mib, *operands):
    return pl.pallas_call(
        function,
        out_shape=[o[0] for o in outs],
        in_specs=specs,
        out_specs=[o[1] for o in outs],
        scratch_shapes=scratch,
        compiler_params=pltpu.CompilerParams(vmem_limit_bytes=mib * 1024 * 1024),
        cost_estimate=pl.CostEstimate(flops=flops, bytes_accessed=8 * 1024 * 1024, transcendentals=0),
    )(*operands)


def per_device(tokens, w_value, w_gate, conv_weight, norm_gain, norm_bias, w_out):
    rows = tokens[0]
    length, depth = rows.shape
    taps, channels = conv_weight.shape
    positions = lax.axis_size(("zh", "zl"))
    core, side, parity = (lax.axis_index(a) for a in ("core", "side", "zl"))
    where = jnp.stack([core, side, parity]).astype(jnp.int32)

    both = jnp.stack([w_value.T, w_gate.T, w_out])
    half = both.shape[1] // 2
    mine = lax.dynamic_slice_in_dim(both, side * half, half, 1)
    far = lax.all_gather(mine, "zh", axis=0, tiled=True)
    own = far.reshape(lax.axis_size("zh"), *mine.shape).transpose(1, 0, 2, 3)
    own = own.reshape(3, -1, mine.shape[-1])
    last = rows[length - HALO :]
    own, last, conv_weight, norm_gain, norm_bias = lax.optimization_barrier((own, last, conv_weight, norm_gain, norm_bias))

    vg = own[:2]
    vg_side = swapped(vg, "side")
    own0 = exchanged(copies(own, "x"), "x")
    vg_zl = swapped(jnp.stack([vg, vg_side]), "zl")
    halo = lax.ppermute(last, ("zh", "zl"), [(i, i + 1) for i in range(positions - 1)])
    rest = jnp.concatenate([vg_side[None], vg_zl], axis=0)
    rest0 = exchanged(copies(rest, "x"), "x")
    o00 = own0[:, 2]
    o10 = swapped(o00, "side")
    o01 = swapped(o00, "zl")
    own1 = swapped(own0, "core")
    o11 = swapped(o01, "side")
    o10c = swapped(o10, "core")
    o01c = swapped(o01, "core")
    o11c = swapped(o11, "core")
    rest1 = swapped(rest0, "core")

    shape, vmem, dma = jax.ShapeDtypeStruct, pltpu.VMEM, pltpu.SemaphoreType.DMA
    part, blocks, deep = channels // 4, own0.shape[0], own0.shape[-1]
    tok = ((length + HALO, depth), jnp.bfloat16)
    cw = ((4, taps, part), jnp.float32)
    stats = (shape((2, length, LANES), jnp.float32), VMEM)
    shifted = vmem((8, length + HALO, part), jnp.float32)
    flops = 2 * length * depth * channels // 2
    conv_a, stats_a, tok_ready, cw_ready = kernel(
        first, [SMEM, HBM, HBM, HBM, ANY, ANY],
        [(shape((length, part), jnp.bfloat16), VMEM), stats, (shape(*tok), HBM), (shape(*cw), HBM)],
        [vmem(*tok), vmem(*cw), vmem((2, blocks, 2, part, deep), jnp.bfloat16), shifted,
         vmem((taps, channels), jnp.bfloat16), dma((5 + 4 * blocks,))],
        flops, 56, where, halo, rows, conv_weight, own0, own1,
    )
    (mixed,) = kernel(
        remaining, [SMEM, HBM, HBM, ANY, ANY, HBM, HBM, HBM, HBM] + [ANY] * 8,
        [(shape((length, depth), jnp.bfloat16), VMEM)],
        [vmem(*tok), vmem(*cw), vmem((3, 2, blocks, 2, part, deep), jnp.bfloat16), shifted,
         vmem((4, length, part), jnp.bfloat16), vmem((length, channels), jnp.bfloat16),
         vmem((2, length, LANES), jnp.float32), vmem((2, length, LANES), jnp.float32),
         vmem((16, channels), jnp.float32), vmem((2, 4, blocks, part, deep), jnp.bfloat16), dma((20,))],
        3 * flops, 56, where, tok_ready, cw_ready, rest0, rest1,
        conv_a, stats_a, norm_gain[None], norm_bias[None],
        own0, o10, o01, o11, own1, o10c, o01c, o11c,
    )
    return mixed[None]


def solution(mesh):
    groups, positions, columns = (mesh.shape[a] for a in ("grp", "sp", "dp"))
    fine = Mesh(
        mesh.devices.reshape(groups // 2, 2, positions // 2, 2, columns // 2, 2),
        ("pair", "side", "zh", "zl", "x", "core"),
    )
    z, dp = ("zh", "zl"), ("x", "core")
    placed = (
        P(("pair", "side", *dp), z, None),
        P(dp, z),
        P(dp, z),
        P(),
        P(),
        P(),
        P(z, dp),
    )
    return jax.shard_map(
        per_device,
        mesh=fine,
        in_specs=placed,
        out_specs=P(("pair", "side", *dp), z, None),
        check_vma=False,
    )
```

profile of v0, /device:TPU:33, one launch (start us, length us, event | category | flops | bytes accessed | tf_op | source)
XLA Modules:
  0.0 217.0 jit_solution(2644420157321037238)
XLA Ops:
  0.0 0.9 slice_bitcast_fusion.1
  0.9 0.7 fusion.1
  1.7 69.0 %all_gather.3 = bf16[48,16,256]{2,1,0:T(8,128)(2,1)S(1)} all-gather(bf16[3,16,256]{2,1,0:T(8,128)(2,1)S(1)} %fusion.1), channel_id=1, replica_groups=mesh['pair'=1,'side'=2,'zh'=16,'zl'=2,'x'=4,'core'=2] {'zh'}, dimensions={0}, use_global_device_ids=true | all-gather | bytes 417792 | tf_op jit(solution)/shard_map/all_gather | solution.py:181
  70.8 4.0 %collective-permute-start.2 = (bf16[2,256,256]{2,1,0:T(8,128)(2,1)S(1)}, bf16[2,256,256]{2,1,0:T(8,128)(2,1)S(1)}, u32[]{:S(2)}, u32[]{:S(2)}) collective-permute-start(bf16[2,256,256]{2,1,0:T(8,128)(2,1)S(1)} %get-tuple-element.24), channel_id=1, source_target_pairs={{0,256},{256,0},{1,257},{257,1},{2,258},{258,2},{3,259},{259,3},{4... | collective-permute-start | bytes 786440 | tf_op jit(solution)/shard_map/ppermute | solution.py:24
  74.8 3.7 %collective-permute-done.2 = bf16[2,256,256]{2,1,0:T(8,128)(2,1)S(1)} collective-permute-done((bf16[2,256,256]{2,1,0:T(8,128)(2,1)S(1)}, bf16[2,256,256]{2,1,0:T(8,128)(2,1)S(1)}, u32[]{:S(2)}, u32[]{:S(2)}) %collective-permute-start.2) | collective-permute-done | bytes 262176 | tf_op jit(solution)/shard_map/ppermute | solution.py:24
  78.6 3.4 %collective-permute-start.3 = (bf16[2,2,256,256]{3,2,1,0:T(8,128)(2,1)S(1)}, bf16[2,2,256,256]{3,2,1,0:T(8,128)(2,1)S(1)}, u32[]{:S(2)}, u32[]{:S(2)}) collective-permute-start(bf16[2,2,256,256]{3,2,1,0:T(8,128)(2,1)S(1)} %pad_maximum_fusion.1), channel_id=1, source_target_pairs={{0,8},{8,0},{1,9},{9,1},{2,10},{10,2},{3,11},{11,3},{4,12},{12,4},... | collective-permute-start | bytes 1572872 | tf_op jit(solution)/shard_map/ppermute | solution.py:24
  82.0 6.6 %collective-permute-done.3 = bf16[2,2,256,256]{3,2,1,0:T(8,128)(2,1)S(1)} collective-permute-done((bf16[2,2,256,256]{3,2,1,0:T(8,128)(2,1)S(1)}, bf16[2,2,256,256]{3,2,1,0:T(8,128)(2,1)S(1)}, u32[]{:S(2)}, u32[]{:S(2)}) %collective-permute-start.3) | collective-permute-done | bytes 524320 | tf_op jit(solution)/shard_map/ppermute | solution.py:24
  88.9 32.5 %all_to_all.10.w0_ref = bf16[4,3,2,256,256]{4,3,2,1,0:T(8,128)(2,1)} all-to-all(bf16[4,3,2,256,256]{4,3,2,1,0:T(8,128)(2,1)S(1)} %broadcast_in_dim.20), channel_id=1, replica_groups=mesh['pair'=1,'side'=2,'zh'=16,'zl'=2,'x'=4,'core'=2] {'x'}, dimensions={0} | all-to-all | bytes 6291456 | tf_op jit(solution)/shard_map/all_to_all | solution.py:20
  121.4 12.2 %collective-permute-start.4 = (bf16[4,3,2,256,256]{4,3,2,1,0:T(8,128)(2,1)}, bf16[4,3,2,256,256]{4,3,2,1,0:T(8,128)(2,1)}, u32[]{:S(2)}, u32[]{:S(2)}) collective-permute-start(bf16[4,3,2,256,256]{4,3,2,1,0:T(8,128)(2,1)} %all_to_all.10.w0_ref), channel_id=1, source_target_pairs={{0,1},{1,0},{2,3},{3,2},{4,5},{5,4},{6,7},{7,6},{8,9},{9,8},{10,11... | collective-permute-start | bytes 9437192 | tf_op jit(solution)/shard_map/ppermute | solution.py:24
  133.7 23.0 %all_to_all.11.w0_ref.refs_0_ = bf16[4,3,256,256]{3,2,1,0:T(8,128)(2,1)S(1)} all-to-all(bf16[4,3,256,256]{3,2,1,0:T(8,128)(2,1)S(1)} %broadcast_in_dim.18), channel_id=1, replica_groups=mesh['pair'=1,'side'=2,'zh'=16,'zl'=2,'x'=4,'core'=2] {'x'}, dimensions={0} | all-to-all | bytes 3145728 | tf_op jit(solution)/shard_map/all_to_all | solution.py:20
  156.7 3.1 %collective-permute-start.1 = (bf16[4,3,256,256]{3,2,1,0:T(8,128)(2,1)S(1)}, bf16[4,3,256,256]{3,2,1,0:T(8,128)(2,1)S(1)}, u32[]{:S(2)}, u32[]{:S(2)}) collective-permute-start(bf16[4,3,256,256]{3,2,1,0:T(8,128)(2,1)S(1)} %all_to_all.11.w0_ref.refs_0_), channel_id=1, source_target_pairs={{0,1},{1,0},{2,3},{3,2},{4,5},{5,4},{6,7},{7,6},{8,9},{9,8},{10,11... | collective-permute-start | bytes 4718600 | tf_op jit(solution)/shard_map/ppermute | solution.py:24
  159.9 3.4 %collective-permute-start.6 = (bf16[4,256,256]{2,1,0:T(8,128)(2,1)S(1)}, bf16[4,256,256]{2,1,0:T(8,128)(2,1)}, u32[]{:S(2)}, u32[]{:S(2)}) collective-permute-start(bf16[4,256,256]{2,1,0:T(8,128)(2,1)S(1)} %slice_bitcast_fusion), channel_id=1, source_target_pairs={{0,8},{8,0},{1,9},{9,1},{2,10},{10,2},{3,11},{11,3},{4,12},{12,4},... | collective-permute-start | bytes 1572872 | tf_op jit(solution)/shard_map/ppermute | solution.py:24
  163.3 3.4 %collective-permute-start.5 = (bf16[4,256,256]{2,1,0:T(8,128)(2,1)S(1)}, bf16[4,256,256]{2,1,0:T(8,128)(2,1)}, u32[]{:S(2)}, u32[]{:S(2)}) collective-permute-start(bf16[4,256,256]{2,1,0:T(8,128)(2,1)S(1)} %slice_bitcast_fusion), channel_id=1, source_target_pairs={{0,256},{256,0},{1,257},{257,1},{2,258},{258,2},{3,259},{259,3},{4... | collective-permute-start | bytes 1572872 | tf_op jit(solution)/shard_map/ppermute | solution.py:24
  166.7 8.7 %collective-permute-done.6.refs_2_ = bf16[4,256,256]{2,1,0:T(8,128)(2,1)} collective-permute-done((bf16[4,256,256]{2,1,0:T(8,128)(2,1)S(1)}, bf16[4,256,256]{2,1,0:T(8,128)(2,1)}, u32[]{:S(2)}, u32[]{:S(2)}) %collective-permute-start.6) | collective-permute-done | bytes 524320 | tf_op jit(solution)/shard_map/ppermute | solution.py:24
  175.4 3.4 %collective-permute-start.7 = (bf16[4,256,256]{2,1,0:T(8,128)(2,1)}, bf16[4,256,256]{2,1,0:T(8,128)(2,1)}, u32[]{:S(2)}, u32[]{:S(2)}) collective-permute-start(bf16[4,256,256]{2,1,0:T(8,128)(2,1)} %collective-permute-done.6.refs_2_), channel_id=1, source_target_pairs={{0,256},{256,0},{1,257},{257,1},{2,258},{258,2},{3,259},{259,3},{4... | collective-permute-start | bytes 1572872 | tf_op jit(solution)/shard_map/ppermute | solution.py:24
  178.8 3.4 %collective-permute-start = (bf16[32,2048]{1,0:T(8,128)(2,1)S(1)}, bf16[32,2048]{1,0:T(8,128)(2,1)S(1)}, u32[]{:S(2)}, u32[]{:S(2)}) collective-permute-start(bf16[32,2048]{1,0:T(8,128)(2,1)S(1)} %slice_bitcast_fusion.1), channel_id=1, source_target_pairs={{0,8},{8,16},{16,24},{24,32},{32,40},{40,48},{48,56},{56,64},{64,7... | collective-permute-start | bytes 393224 | tf_op jit(solution)/shard_map/ppermute | solution.py:191
  182.2 1.9 collective-permute-done.halo_ref
  184.1 3.9 %collective-permute-start.9 = (bf16[4,256,256]{2,1,0:T(8,128)(2,1)}, bf16[4,256,256]{2,1,0:T(8,128)(2,1)}, u32[]{:S(2)}, u32[]{:S(2)}) collective-permute-start(bf16[4,256,256]{2,1,0:T(8,128)(2,1)} %collective-permute-done.6.refs_2_), channel_id=1, source_target_pairs={{0,1},{1,0},{2,3},{3,2},{4,5},{5,4},{6,7},{7,6},{8,9},{9,8},{10,11... | collective-permute-start | bytes 1572872 | tf_op jit(solution)/shard_map/ppermute | solution.py:24
  188.0 2.0 collective-permute-start.8
  190.2 3.8 %collective-permute-start.10 = (bf16[4,256,256]{2,1,0:T(8,128)(2,1)}, bf16[4,256,256]{2,1,0:T(8,128)(2,1)}, u32[]{:S(2)}, u32[]{:S(2)}) collective-permute-start(bf16[4,256,256]{2,1,0:T(8,128)(2,1)} %collective-permute-done.7.refs_3_), channel_id=1, source_target_pairs={{0,1},{1,0},{2,3},{3,2},{4,5},{5,4},{6,7},{7,6},{8,9},{9,8},{10,11... | collective-permute-start | bytes 1572872 | tf_op jit(solution)/shard_map/ppermute | solution.py:24
  194.1 0.6 pad_add_fusion.where_ref
  194.7 1.1 copy-done.1
  195.8 6.1 %shard_map.73 = (bf16[384,256]{1,0:T(8,128)(2,1)}, f32[2,384,128]{2,1,0:T(8,128)}, bf16[416,2048]{1,0:T(8,128)(2,1)}, f32[4,31,256]{2,1,0:T(8,128)}) custom-call(s32[3]{0:T(128)} %pad_add_fusion.where_ref, bf16[32,2048]{1,0:T(8,128)(2,1)} %copy-done.2, bf16[384,2048]{1,0:T(8,128)(2,1)} %bitcast.29, bf16[31,1024]{1,0:T(8,128)(2,1)} %cw_ref, ...), custom_call_target="tpu_custom_call" | custom-call | flops 805306368 | bytes 8388608 | tf_op jit(solution)/shard_map/pallas_call | solution.py:159
  202.0 14.9 %shard_map.74 = bf16[384,2048]{1,0:T(8,128)(2,1)} custom-call(s32[3]{0:T(128)} %pad_add_fusion.where_ref, bf16[416,2048]{1,0:T(8,128)(2,1)} %get-tuple-element.17.tok_ref, f32[4,31,256]{2,1,0:T(8,128)} %get-tuple-element.18.cw_ref, bf16[4,3,2,256,256]{4,3,2,1,0:T(8,128)(2,1)} %all_to_all.10.w0_ref, ...), custom_call_target="tpu_custom_call" | custom-call | flops 2415919104 | bytes 8388608 | tf_op jit(solution)/shard_map/pallas_call | solution.py:159
  (19 shorter events, 0.9 us)
Async XLA Ops:
  70.8 7.7 %collective-permute-start.2 = (bf16[2,256,256]{2,1,0:T(8,128)(2,1)S(1)}, bf16[2,256,256]{2,1,0:T(8,128)(2,1)S(1)}, u32[]{:S(2)}, u32[]{:S(2)}) collective-permute-start(bf16[2,256,256]{2,1,0:T(8,128)(2,1)S(1)} %get-tuple-element.24), channel_id=1, source_target_pairs={{0,256},{256,0},{1,257},{257,1},{2,258},{258,2},{3,259},{259,3},{4... | collective-permute-start | bytes 786440 | tf_op jit(solution)/shard_map/ppermute | solution.py:24
  78.6 10.0 %collective-permute-start.3 = (bf16[2,2,256,256]{3,2,1,0:T(8,128)(2,1)S(1)}, bf16[2,2,256,256]{3,2,1,0:T(8,128)(2,1)S(1)}, u32[]{:S(2)}, u32[]{:S(2)}) collective-permute-start(bf16[2,2,256,256]{3,2,1,0:T(8,128)(2,1)S(1)} %pad_maximum_fusion.1), channel_id=1, source_target_pairs={{0,8},{8,0},{1,9},{9,1},{2,10},{10,2},{3,11},{11,3},{4,12},{12,4},... | collective-permute-start | bytes 1572872 | tf_op jit(solution)/shard_map/ppermute | solution.py:24
  121.4 80.6 %collective-permute-start.4 = (bf16[4,3,2,256,256]{4,3,2,1,0:T(8,128)(2,1)}, bf16[4,3,2,256,256]{4,3,2,1,0:T(8,128)(2,1)}, u32[]{:S(2)}, u32[]{:S(2)}) collective-permute-start(bf16[4,3,2,256,256]{4,3,2,1,0:T(8,128)(2,1)} %all_to_all.10.w0_ref), channel_id=1, source_target_pairs={{0,1},{1,0},{2,3},{3,2},{4,5},{5,4},{6,7},{7,6},{8,9},{9,8},{10,11... | collective-permute-start | bytes 9437192 | tf_op jit(solution)/shard_map/ppermute | solution.py:24
  156.7 38.0 %copy-start = (bf16[4,3,256,256]{3,2,1,0:T(8,128)(2,1)}, bf16[4,3,256,256]{3,2,1,0:T(8,128)(2,1)S(1)}, u32[]{:S(2)}) copy-start(bf16[4,3,256,256]{3,2,1,0:T(8,128)(2,1)S(1)} %all_to_all.11.w0_ref.refs_0_) | copy-start | bytes 4718596
  156.7 38.0 %collective-permute-start.1 = (bf16[4,3,256,256]{3,2,1,0:T(8,128)(2,1)S(1)}, bf16[4,3,256,256]{3,2,1,0:T(8,128)(2,1)S(1)}, u32[]{:S(2)}, u32[]{:S(2)}) collective-permute-start(bf16[4,3,256,256]{3,2,1,0:T(8,128)(2,1)S(1)} %all_to_all.11.w0_ref.refs_0_), channel_id=1, source_target_pairs={{0,1},{1,0},{2,3},{3,2},{4,5},{5,4},{6,7},{7,6},{8,9},{9,8},{10,11... | collective-permute-start | bytes 4718600 | tf_op jit(solution)/shard_map/ppermute | solution.py:24
  159.9 15.5 %collective-permute-start.6 = (bf16[4,256,256]{2,1,0:T(8,128)(2,1)S(1)}, bf16[4,256,256]{2,1,0:T(8,128)(2,1)}, u32[]{:S(2)}, u32[]{:S(2)}) collective-permute-start(bf16[4,256,256]{2,1,0:T(8,128)(2,1)S(1)} %slice_bitcast_fusion), channel_id=1, source_target_pairs={{0,8},{8,0},{1,9},{9,1},{2,10},{10,2},{3,11},{11,3},{4,12},{12,4},... | collective-permute-start | bytes 1572872 | tf_op jit(solution)/shard_map/ppermute | solution.py:24
  163.3 24.8 %collective-permute-start.5 = (bf16[4,256,256]{2,1,0:T(8,128)(2,1)S(1)}, bf16[4,256,256]{2,1,0:T(8,128)(2,1)}, u32[]{:S(2)}, u32[]{:S(2)}) collective-permute-start(bf16[4,256,256]{2,1,0:T(8,128)(2,1)S(1)} %slice_bitcast_fusion), channel_id=1, source_target_pairs={{0,256},{256,0},{1,257},{257,1},{2,258},{258,2},{3,259},{259,3},{4... | collective-permute-start | bytes 1572872 | tf_op jit(solution)/shard_map/ppermute | solution.py:24
  175.4 14.8 %collective-permute-start.7 = (bf16[4,256,256]{2,1,0:T(8,128)(2,1)}, bf16[4,256,256]{2,1,0:T(8,128)(2,1)}, u32[]{:S(2)}, u32[]{:S(2)}) collective-permute-start(bf16[4,256,256]{2,1,0:T(8,128)(2,1)} %collective-permute-done.6.refs_2_), channel_id=1, source_target_pairs={{0,256},{256,0},{1,257},{257,1},{2,258},{258,2},{3,259},{259,3},{4... | collective-permute-start | bytes 1572872 | tf_op jit(solution)/shard_map/ppermute | solution.py:24
  178.8 5.3 %collective-permute-start = (bf16[32,2048]{1,0:T(8,128)(2,1)S(1)}, bf16[32,2048]{1,0:T(8,128)(2,1)S(1)}, u32[]{:S(2)}, u32[]{:S(2)}) collective-permute-start(bf16[32,2048]{1,0:T(8,128)(2,1)S(1)} %slice_bitcast_fusion.1), channel_id=1, source_target_pairs={{0,8},{8,16},{16,24},{24,32},{32,40},{40,48},{48,56},{56,64},{64,7... | collective-permute-start | bytes 393224 | tf_op jit(solution)/shard_map/ppermute | solution.py:191
  184.1 10.6 %copy-start.2 = (bf16[32,2048]{1,0:T(8,128)(2,1)}, bf16[32,2048]{1,0:T(8,128)(2,1)S(1)}, u32[]{:S(2)}) copy-start(bf16[32,2048]{1,0:T(8,128)(2,1)S(1)} %collective-permute-done.halo_ref) | copy-start | bytes 393220
  184.1 17.9 %collective-permute-start.9 = (bf16[4,256,256]{2,1,0:T(8,128)(2,1)}, bf16[4,256,256]{2,1,0:T(8,128)(2,1)}, u32[]{:S(2)}, u32[]{:S(2)}) collective-permute-start(bf16[4,256,256]{2,1,0:T(8,128)(2,1)} %collective-permute-done.6.refs_2_), channel_id=1, source_target_pairs={{0,1},{1,0},{2,3},{3,2},{4,5},{5,4},{6,7},{7,6},{8,9},{9,8},{10,11... | collective-permute-start | bytes 1572872 | tf_op jit(solution)/shard_map/ppermute | solution.py:24
  188.0 14.0 %collective-permute-start.8 = (bf16[4,256,256]{2,1,0:T(8,128)(2,1)}, bf16[4,256,256]{2,1,0:T(8,128)(2,1)}, u32[]{:S(2)}, u32[]{:S(2)}) collective-permute-start(bf16[4,256,256]{2,1,0:T(8,128)(2,1)} %collective-permute-done.5.refs_1_), channel_id=1, source_target_pairs={{0,1},{1,0},{2,3},{3,2},{4,5},{5,4},{6,7},{7,6},{8,9},{9,8},{10,11... | collective-permute-start | bytes 1572872 | tf_op jit(solution)/shard_map/ppermute | solution.py:24
  190.2 11.8 %collective-permute-start.10 = (bf16[4,256,256]{2,1,0:T(8,128)(2,1)}, bf16[4,256,256]{2,1,0:T(8,128)(2,1)}, u32[]{:S(2)}, u32[]{:S(2)}) collective-permute-start(bf16[4,256,256]{2,1,0:T(8,128)(2,1)} %collective-permute-done.7.refs_3_), channel_id=1, source_target_pairs={{0,1},{1,0},{2,3},{3,2},{4,5},{5,4},{6,7},{7,6},{8,9},{9,8},{10,11... | collective-permute-start | bytes 1572872 | tf_op jit(solution)/shard_map/ppermute | solution.py:24
  194.7 1.1 copy-start.1
where the time goes:
time: 218 us; the launch traced here: 217 us
  blocking collectives  124 us (57%)
  starting transfers between devices  45.9 us (21%)
  waiting for transfers between devices  21.2 us (10%)
  Pallas kernels  21 us (10%)
  local copies, waits for them, and re-layouts  2.61 us (1%)
    all_gather x1, blocking collectives, per_device(): far = lax.all_gather(mine, 'zh', axis=0, tiled=True)  69 us
    all_to_all x2, blocking collectives, exchanged(): return lax.all_to_all(blocks, axis, 0, 0)  55.4 us
    ppermute x10, starting transfers between devices, swapped(): return lax.ppermute(array, axis, [(0, 1), (1, 0)])  42.5 us
    pallas_call x2, Pallas kernels, kernel(): pl.pallas_call(function, out_shape=[o[0] for o in outs], in_specs=specs,...  21 us
    ppermute x10, waiting for transfers between devices, swapped(): return lax.ppermute(array, axis, [(0, 1), (1, 0)])  19.2 us
  transfers between devices with their start and end apart: 11, of which 5 were waited for; matrix products, arithmetic and copies ran while one was open for 0% of the time, Pallas kernels for 3%

commit v1 on v0

--- a/solution.py
+++ b/solution.py
@@ -79,24 +79,38 @@
     return jnp.concatenate([w[(m, x, *index)] for x in range(blocks) for m in range(2)], axis=1)
 
 
-def first(where_ref, halo_ref, tok_ref, cw_ref, w0_ref, w1_ref, conv_ref, stats_ref, tok_out, cw_out, tok, cw, w, shifted, taps, sems):
+def first(
+    where_ref, halo_ref, tok_ref, cw_ref, gain_ref, bias_ref, w0_ref, w1_ref, conv_ref, stats_ref, tok_out, cw_out, affine_out,
+    tok, cw, w, shifted, taps, raw, affine, sems,
+):
     blocks = w.shape[1]
     rows, deep = tok_ref.shape[0], tok.shape[1] // (2 * blocks)
     loads = [pltpu.make_async_copy(cw_ref, taps, sems.at[0])]
     for at in range(2 * blocks):
         here, there = pl.ds(at * deep, deep), columns(where_ref, at // 2, at % 2, deep)
-        loads.append(pltpu.make_async_copy(halo_ref.at[:, there], tok.at[pl.ds(0, HALO), here], sems.at[5 + 2 * at]))
-        loads.append(pltpu.make_async_copy(tok_ref.at[:, there], tok.at[pl.ds(HALO, rows), here], sems.at[6 + 2 * at]))
+        loads.append(pltpu.make_async_copy(halo_ref.at[:, there], tok.at[pl.ds(0, HALO), here], sems.at[8 + 2 * at]))
+        loads.append(pltpu.make_async_copy(tok_ref.at[:, there], tok.at[pl.ds(HALO, rows), here], sems.at[9 + 2 * at]))
     for m, r in enumerate((w0_ref, w1_ref)):
         loads.append(pltpu.make_async_copy(r.at[:, pl.ds(0, 2)], w.at[m], sems.at[1 + m]))
+    loads.append(pltpu.make_async_copy(gain_ref, raw.at[pl.ds(0, 1)], sems.at[5]))
+    loads.append(pltpu.make_async_copy(bias_ref, raw.at[pl.ds(8, 1)], sems.at[6]))
     for load in loads:
         load.start()
     loads[0].wait()
+    loads[-2].wait()
+    loads[-1].wait()
+    pair = jnp.concatenate([raw[0:1], raw[8:9], jnp.zeros((6, raw.shape[1]), jnp.float32)], axis=0)
+    part = cw.shape[2]
     for i, quarter in enumerate(QUARTERS):
         cw[i] = chosen(taps[...], where_ref, quarter)
-    for load in loads[1:]:
+        affine[:, i * part : (i + 1) * part] = chosen(pair, where_ref, quarter, lax.Precision.HIGHEST)
+    for load in loads[1:-2]:
         load.wait()
-    stores = [pltpu.make_async_copy(tok, tok_out, sems.at[3]), pltpu.make_async_copy(cw, cw_out, sems.at[4])]
+    stores = [
+        pltpu.make_async_copy(tok, tok_out, sems.at[3]),
+        pltpu.make_async_copy(cw, cw_out, sems.at[4]),
+        pltpu.make_async_copy(affine, affine_out, sems.at[7]),
+    ]
     for store in stores:
         store.start()
     convolve(True, tok, cw.at[pl.ds(0, 1)], joined(w, blocks, 0), joined(w, blocks, 1), conv_ref, stats_ref, shifted)
@@ -104,52 +118,60 @@
         store.wait()
 
 
-def remaining(where_ref, tok_ref, cw_ref, w0_ref, w1_ref, first_ref, stats_ref, gain_ref, bias_ref, *refs):
-    o_refs, (out_ref, tok, cw, w, shifted, conv, whole, stats, more, affine, o, sems) = refs[:-12], refs[-12:]
+def remaining(where_ref, tok_ref, cw_ref, affine_ref, w0_ref, w1_ref, first_ref, stats_ref, *refs):
+    o_refs, (out_ref, tok, cw, w, shifted, conv, whole, stats, more, affine, o, out, sems) = refs[:-13], refs[-13:]
     count, blocks, part, deep = w.shape[0], w.shape[2], w.shape[4], w.shape[5]
     channels = whole.shape[1]
     serial = iter(range(64))
 
     def load(source, target):
-        copy = pltpu.make_async_copy(source, target, sems.at[next(serial)])
-        copy.start()
-        return copy
+        return pltpu.make_async_copy(source, target, sems.at[next(serial)])
+
+    def start(loads):
+        for copy in loads:
+            copy.start()
+
+    def wait(loads):
+        for copy in loads:
+            copy.wait()
 
     early = [load(tok_ref, tok), load(cw_ref, cw)]
     pieces = [[load(r.at[:, i], w.at[i, m]) for m, r in enumerate((w0_ref, w1_ref))] for i in range(count)]
-    middle = [load(first_ref, conv.at[0]), load(stats_ref, stats)]
-    middle += [load(gain_ref, affine.at[pl.ds(0, 1)]), load(bias_ref, affine.at[pl.ds(8, 1)])]
+    middle = [load(first_ref, conv.at[0]), load(stats_ref, stats), load(affine_ref, affine)]
     late = []
     for i, r in enumerate(o_refs):
         m, q = i // len(QUARTERS), i % len(QUARTERS)
         late.append(load(r.at[:, 2] if q == 0 else r, o.at[m, q]))
-    for copy in early:
-        copy.wait()
+    start(early + pieces[0])
+    wait(early + pieces[0])
+    start(sum(pieces[1:], []) + middle)
     for i in range(count):
-        for copy in pieces[i]:
-            copy.wait()
+        if i == 1:
+            wait(pieces[1])
+            start(late)
+        elif i > 1:
+            wait(pieces[i])
         piece = w.at[i]
         value, gate = joined(piece, blocks, 0), joined(piece, blocks, 1)
         convolve(i == 0, tok, cw.at[pl.ds(1 + i, 1)], value, gate, conv.at[1 + i], more, shifted)
-    for copy in middle:
-        copy.wait()
+    wait(middle)
     mean = jnp.sum(stats[0] + more[0], axis=1, keepdims=True) / channels
     meansq = jnp.sum(stats[1] + more[1], axis=1, keepdims=True) / channels
     scale = lax.rsqrt(meansq - mean * mean + EPS)
-    for q, quarter in enumerate(QUARTERS):
-        gain, bias = (
-            chosen(jnp.broadcast_to(affine[at : at + 1], (8, channels)), where_ref, quarter, lax.Precision.HIGHEST)[:1]
-            for at in (0, 8)
-        )
-        v = (conv[q].astype(jnp.float32) - mean) * scale * gain + bias
-        whole[:, q * part : (q + 1) * part] = (v / (1.0 + jnp.exp(-v))).astype(jnp.bfloat16)
-    for copy in late:
-        copy.wait()
+    for q in range(len(QUARTERS)):
+        here = slice(q * part, (q + 1) * part)
+        v = (conv[q].astype(jnp.float32) - mean) * scale * affine[0:1, here] + affine[1:2, here]
+        whole[:, here] = (v / (1.0 + jnp.exp(-v))).astype(jnp.bfloat16)
+    wait(late)
+    stores = []
     for x in range(blocks):
         for m in range(2):
             right = jnp.concatenate([o[m, q, x] for q in range(len(QUARTERS))], axis=0)
-            out = jnp.dot(whole[...], right, preferred_element_type=jnp.float32)
-            out_ref[:, columns(where_ref, x, m, deep)] = out.astype(jnp.bfloat16)
+            at = 2 * x + m
+            out[at] = jnp.dot(whole[...], right, preferred_element_type=jnp.float32).astype(jnp.bfloat16)
+            stores.append(load(out.at[at], out_ref.at[:, columns(where_ref, x, m, deep)]))
+            stores[-1].start()
+    wait(stores)
 
 
 SMEM, VMEM, HBM, ANY = (pl.BlockSpec(memory_space=space) for space in (pltpu.SMEM, pltpu.VMEM, pltpu.HBM, pl.ANY))
@@ -181,13 +203,12 @@
     far = lax.all_gather(mine, "zh", axis=0, tiled=True)
     own = far.reshape(lax.axis_size("zh"), *mine.shape).transpose(1, 0, 2, 3)
     own = own.reshape(3, -1, mine.shape[-1])
-    last = rows[length - HALO :]
-    own, last, conv_weight, norm_gain, norm_bias = lax.optimization_barrier((own, last, conv_weight, norm_gain, norm_bias))
 
     vg = own[:2]
     vg_side = swapped(vg, "side")
     own0 = exchanged(copies(own, "x"), "x")
     vg_zl = swapped(jnp.stack([vg, vg_side]), "zl")
+    last = rows[length - HALO :]
     halo = lax.ppermute(last, ("zh", "zl"), [(i, i + 1) for i in range(positions - 1)])
     rest = jnp.concatenate([vg_side[None], vg_zl], axis=0)
     rest0 = exchanged(copies(rest, "x"), "x")
@@ -208,22 +229,24 @@
     stats = (shape((2, length, LANES), jnp.float32), VMEM)
     shifted = vmem((8, length + HALO, part), jnp.float32)
     flops = 2 * length * depth * channels // 2
-    conv_a, stats_a, tok_ready, cw_ready = kernel(
-        first, [SMEM, HBM, HBM, HBM, ANY, ANY],
-        [(shape((length, part), jnp.bfloat16), VMEM), stats, (shape(*tok), HBM), (shape(*cw), HBM)],
+    conv_a, stats_a, tok_ready, cw_ready, affine = kernel(
+        first, [SMEM] + [HBM] * 5 + [ANY] * 2,
+        [(shape((length, part), jnp.bfloat16), VMEM), stats, (shape(*tok), HBM), (shape(*cw), HBM),
+         (shape((8, channels), jnp.float32), HBM)],
         [vmem(*tok), vmem(*cw), vmem((2, blocks, 2, part, deep), jnp.bfloat16), shifted,
-         vmem((taps, channels), jnp.bfloat16), dma((5 + 4 * blocks,))],
-        flops, 56, where, halo, rows, conv_weight, own0, own1,
+         vmem((taps, channels), jnp.bfloat16), vmem((16, channels), jnp.float32),
+         vmem((8, channels), jnp.float32), dma((8 + 4 * blocks,))],
+        flops, 56, where, halo, rows, conv_weight, norm_gain[None], norm_bias[None], own0, own1,
     )
     (mixed,) = kernel(
-        remaining, [SMEM, HBM, HBM, ANY, ANY, HBM, HBM, HBM, HBM] + [ANY] * 8,
-        [(shape((length, depth), jnp.bfloat16), VMEM)],
+        remaining, [SMEM, HBM, HBM, HBM, ANY, ANY, HBM, HBM] + [ANY] * 8,
+        [(shape((length, depth), jnp.bfloat16), HBM)],
         [vmem(*tok), vmem(*cw), vmem((3, 2, blocks, 2, part, deep), jnp.bfloat16), shifted,
          vmem((4, length, part), jnp.bfloat16), vmem((length, channels), jnp.bfloat16),
          vmem((2, length, LANES), jnp.float32), vmem((2, length, LANES), jnp.float32),
-         vmem((16, channels), jnp.float32), vmem((2, 4, blocks, part, deep), jnp.bfloat16), dma((20,))],
-        3 * flops, 56, where, tok_ready, cw_ready, rest0, rest1,
-        conv_a, stats_a, norm_gain[None], norm_bias[None],
+         vmem((8, channels), jnp.float32), vmem((2, 4, blocks, part, deep), jnp.bfloat16),
+         vmem((2 * blocks, length, deep), jnp.bfloat16), dma((32,))],
+        3 * flops, 56, where, tok_ready, cw_ready, affine, rest0, rest1, conv_a, stats_a,
         own0, o10, o01, o11, own1, o10c, o01c, o11c,
     )
     return mixed[None]

time: 218 us -> 216 us (level)
  transfers between devices with their start and end apart: 11 -> 11, of which waited for: 5 -> 4; matrix products, arithmetic and copies ran while one was open for 0% -> 1% of each run, Pallas kernels for 3% -> 3%
where the time goes in v1:
time: 216 us; the launch traced here: 215 us
  blocking collectives  124 us (57%)
  starting transfers between devices  45.2 us (21%)
  waiting for transfers between devices  20.9 us (10%)
  Pallas kernels  20.3 us (9%)
  local copies, waits for them, and re-layouts  2.62 us (1%)
    all_gather x1, blocking collectives, per_device(): far = lax.all_gather(mine, 'zh', axis=0, tiled=True)  69 us
    all_to_all x2, blocking collectives, exchanged(): return lax.all_to_all(blocks, axis, 0, 0)  55.4 us
    ppermute x10, starting transfers between devices, swapped(): return lax.ppermute(array, axis, [(0, 1), (1, 0)])  41.8 us
    pallas_call x2, Pallas kernels, kernel(): pl.pallas_call(function, out_shape=[o[0] for o in outs], in_specs=specs,...  20.3 us
    ppermute x10, waiting for transfers between devices, swapped(): return lax.ppermute(array, axis, [(0, 1), (1, 0)])  19 us
  transfers between devices with their start and end apart: 11, of which 4 were waited for; matrix products, arithmetic and copies ran while one was open for 1% of the time, Pallas kernels for 3%

profile of v1, /device:TPU:33, one launch (start us, length us, event | category | flops | bytes accessed | tf_op | source)
XLA Modules:
  0.0 215.5 jit_solution(18166748151170097041)
XLA Ops:
  0.0 0.7 fusion.1
  0.7 69.0 %all_gather.3 = bf16[48,16,256]{2,1,0:T(8,128)(2,1)S(1)} all-gather(bf16[3,16,256]{2,1,0:T(8,128)(2,1)S(1)} %fusion.1), channel_id=1, replica_groups=mesh['pair'=1,'side'=2,'zh'=16,'zl'=2,'x'=4,'core'=2] {'zh'}, dimensions={0}, use_global_device_ids=true | all-gather | bytes 417792 | tf_op jit(solution)/shard_map/all_gather | solution.py:203
  69.8 4.0 %collective-permute-start.2 = (bf16[2,256,256]{2,1,0:T(8,128)(2,1)S(1)}, bf16[2,256,256]{2,1,0:T(8,128)(2,1)S(1)}, u32[]{:S(2)}, u32[]{:S(2)}) collective-permute-start(bf16[2,256,256]{2,1,0:T(8,128)(2,1)S(1)} %bitcast.31), channel_id=1, source_target_pairs={{0,256},{256,0},{1,257},{257,1},{2,258},{258,2},{3,259},{259,3},{4... | collective-permute-start | bytes 786440 | tf_op jit(solution)/shard_map/ppermute | solution.py:24
  73.8 3.7 %collective-permute-done.2 = bf16[2,256,256]{2,1,0:T(8,128)(2,1)S(1)} collective-permute-done((bf16[2,256,256]{2,1,0:T(8,128)(2,1)S(1)}, bf16[2,256,256]{2,1,0:T(8,128)(2,1)S(1)}, u32[]{:S(2)}, u32[]{:S(2)}) %collective-permute-start.2) | collective-permute-done | bytes 262176 | tf_op jit(solution)/shard_map/ppermute | solution.py:24
  77.6 3.4 %collective-permute-start.3 = (bf16[2,2,256,256]{3,2,1,0:T(8,128)(2,1)S(1)}, bf16[2,2,256,256]{3,2,1,0:T(8,128)(2,1)S(1)}, u32[]{:S(2)}, u32[]{:S(2)}) collective-permute-start(bf16[2,2,256,256]{3,2,1,0:T(8,128)(2,1)S(1)} %pad_maximum_fusion.1), channel_id=1, source_target_pairs={{0,8},{8,0},{1,9},{9,1},{2,10},{10,2},{3,11},{11,3},{4,12},{12,4},... | collective-permute-start | bytes 1572872 | tf_op jit(solution)/shard_map/ppermute | solution.py:24
  81.0 6.6 %collective-permute-done.3 = bf16[2,2,256,256]{3,2,1,0:T(8,128)(2,1)S(1)} collective-permute-done((bf16[2,2,256,256]{3,2,1,0:T(8,128)(2,1)S(1)}, bf16[2,2,256,256]{3,2,1,0:T(8,128)(2,1)S(1)}, u32[]{:S(2)}, u32[]{:S(2)}) %collective-permute-start.3) | collective-permute-done | bytes 524320 | tf_op jit(solution)/shard_map/ppermute | solution.py:24
  88.0 32.5 %all_to_all.10.w0_ref = bf16[4,3,2,256,256]{4,3,2,1,0:T(8,128)(2,1)} all-to-all(bf16[4,3,2,256,256]{4,3,2,1,0:T(8,128)(2,1)S(1)} %broadcast_in_dim.22), channel_id=1, replica_groups=mesh['pair'=1,'side'=2,'zh'=16,'zl'=2,'x'=4,'core'=2] {'x'}, dimensions={0} | all-to-all | bytes 6291456 | tf_op jit(solution)/shard_map/all_to_all | solution.py:20
  120.4 12.2 %collective-permute-start.4 = (bf16[4,3,2,256,256]{4,3,2,1,0:T(8,128)(2,1)}, bf16[4,3,2,256,256]{4,3,2,1,0:T(8,128)(2,1)}, u32[]{:S(2)}, u32[]{:S(2)}) collective-permute-start(bf16[4,3,2,256,256]{4,3,2,1,0:T(8,128)(2,1)} %all_to_all.10.w0_ref), channel_id=1, source_target_pairs={{0,1},{1,0},{2,3},{3,2},{4,5},{5,4},{6,7},{7,6},{8,9},{9,8},{10,11... | collective-permute-start | bytes 9437192 | tf_op jit(solution)/shard_map/ppermute | solution.py:24
  132.8 23.0 %all_to_all.11.w0_ref.refs_0_ = bf16[4,3,256,256]{3,2,1,0:T(8,128)(2,1)S(1)} all-to-all(bf16[4,3,256,256]{3,2,1,0:T(8,128)(2,1)S(1)} %broadcast_in_dim.20), channel_id=1, replica_groups=mesh['pair'=1,'side'=2,'zh'=16,'zl'=2,'x'=4,'core'=2] {'x'}, dimensions={0} | all-to-all | bytes 3145728 | tf_op jit(solution)/shard_map/all_to_all | solution.py:20
  155.8 3.1 %collective-permute-start.1 = (bf16[4,3,256,256]{3,2,1,0:T(8,128)(2,1)S(1)}, bf16[4,3,256,256]{3,2,1,0:T(8,128)(2,1)S(1)}, u32[]{:S(2)}, u32[]{:S(2)}) collective-permute-start(bf16[4,3,256,256]{3,2,1,0:T(8,128)(2,1)S(1)} %all_to_all.11.w0_ref.refs_0_), channel_id=1, source_target_pairs={{0,1},{1,0},{2,3},{3,2},{4,5},{5,4},{6,7},{7,6},{8,9},{9,8},{10,11... | collective-permute-start | bytes 4718600 | tf_op jit(solution)/shard_map/ppermute | solution.py:24
  158.9 3.4 %collective-permute-start.6 = (bf16[4,256,256]{2,1,0:T(8,128)(2,1)S(1)}, bf16[4,256,256]{2,1,0:T(8,128)(2,1)}, u32[]{:S(2)}, u32[]{:S(2)}) collective-permute-start(bf16[4,256,256]{2,1,0:T(8,128)(2,1)S(1)} %slice_bitcast_fusion), channel_id=1, source_target_pairs={{0,8},{8,0},{1,9},{9,1},{2,10},{10,2},{3,11},{11,3},{4,12},{12,4},... | collective-permute-start | bytes 1572872 | tf_op jit(solution)/shard_map/ppermute | solution.py:24
  162.3 3.4 %collective-permute-start.5 = (bf16[4,256,256]{2,1,0:T(8,128)(2,1)S(1)}, bf16[4,256,256]{2,1,0:T(8,128)(2,1)}, u32[]{:S(2)}, u32[]{:S(2)}) collective-permute-start(bf16[4,256,256]{2,1,0:T(8,128)(2,1)S(1)} %slice_bitcast_fusion), channel_id=1, source_target_pairs={{0,256},{256,0},{1,257},{257,1},{2,258},{258,2},{3,259},{259,3},{4... | collective-permute-start | bytes 1572872 | tf_op jit(solution)/shard_map/ppermute | solution.py:24
  165.7 8.7 %collective-permute-done.6.refs_2_ = bf16[4,256,256]{2,1,0:T(8,128)(2,1)} collective-permute-done((bf16[4,256,256]{2,1,0:T(8,128)(2,1)S(1)}, bf16[4,256,256]{2,1,0:T(8,128)(2,1)}, u32[]{:S(2)}, u32[]{:S(2)}) %collective-permute-start.6) | collective-permute-done | bytes 524320 | tf_op jit(solution)/shard_map/ppermute | solution.py:24
  174.4 3.4 %collective-permute-start.7 = (bf16[4,256,256]{2,1,0:T(8,128)(2,1)}, bf16[4,256,256]{2,1,0:T(8,128)(2,1)}, u32[]{:S(2)}, u32[]{:S(2)}) collective-permute-start(bf16[4,256,256]{2,1,0:T(8,128)(2,1)} %collective-permute-done.6.refs_2_), channel_id=1, source_target_pairs={{0,256},{256,0},{1,257},{257,1},{2,258},{258,2},{3,259},{259,3},{4... | collective-permute-start | bytes 1572872 | tf_op jit(solution)/shard_map/ppermute | solution.py:24
  177.8 0.9 slice_bitcast_fusion.1
  178.8 3.4 %collective-permute-start = (bf16[32,2048]{1,0:T(8,128)(2,1)S(1)}, bf16[32,2048]{1,0:T(8,128)(2,1)S(1)}, u32[]{:S(2)}, u32[]{:S(2)}) collective-permute-start(bf16[32,2048]{1,0:T(8,128)(2,1)S(1)} %slice_bitcast_fusion.1), channel_id=1, source_target_pairs={{0,8},{8,16},{16,24},{24,32},{32,40},{40,48},{48,56},{56,64},{64,7... | collective-permute-start | bytes 393224 | tf_op jit(solution)/shard_map/ppermute | solution.py:212
  182.2 1.9 collective-permute-done.halo_ref
  184.1 3.9 %collective-permute-start.9 = (bf16[4,256,256]{2,1,0:T(8,128)(2,1)}, bf16[4,256,256]{2,1,0:T(8,128)(2,1)}, u32[]{:S(2)}, u32[]{:S(2)}) collective-permute-start(bf16[4,256,256]{2,1,0:T(8,128)(2,1)} %collective-permute-done.6.refs_2_), channel_id=1, source_target_pairs={{0,1},{1,0},{2,3},{3,2},{4,5},{5,4},{6,7},{7,6},{8,9},{9,8},{10,11... | collective-permute-start | bytes 1572872 | tf_op jit(solution)/shard_map/ppermute | solution.py:24
  188.0 2.0 collective-permute-start.8
  190.0 3.1 %collective-permute-start.10 = (bf16[4,256,256]{2,1,0:T(8,128)(2,1)}, bf16[4,256,256]{2,1,0:T(8,128)(2,1)}, u32[]{:S(2)}, u32[]{:S(2)}) collective-permute-start(bf16[4,256,256]{2,1,0:T(8,128)(2,1)} %collective-permute-done.7.refs_3_), channel_id=1, source_target_pairs={{0,1},{1,0},{2,3},{3,2},{4,5},{5,4},{6,7},{7,6},{8,9},{9,8},{10,11... | collective-permute-start | bytes 1572872 | tf_op jit(solution)/shard_map/ppermute | solution.py:24
  193.1 0.6 pad_add_fusion.where_ref
  193.8 1.1 copy-done.1
  194.9 7.2 %shard_map.73 = (bf16[384,256]{1,0:T(8,128)(2,1)}, f32[2,384,128]{2,1,0:T(8,128)}, bf16[416,2048]{1,0:T(8,128)(2,1)}, f32[4,31,256]{2,1,0:T(8,128)}, f32[8,1024]{1,0:T(8,128)}) custom-call(s32[3]{0:T(128)} %pad_add_fusion.where_ref, bf16[32,2048]{1,0:T(8,128)(2,1)} %copy-done.2, bf16[384,2048]{1,0:T(8,128)(2,1)} %bitcast.29, bf16[31,1024]{1,0:T(8,128)(2,1)} %cw_ref.1, ...), custom_call_target="tpu_custom_call" | custom-call | flops 805306368 | bytes 8388608 | tf_op jit(solution)/shard_map/pallas_call | solution.py:181
  202.2 13.1 %shard_map.74 = bf16[384,2048]{1,0:T(8,128)(2,1)} custom-call(s32[3]{0:T(128)} %pad_add_fusion.where_ref, bf16[416,2048]{1,0:T(8,128)(2,1)} %get-tuple-element.10.tok_ref, f32[4,31,256]{2,1,0:T(8,128)} %get-tuple-element.11.cw_ref, f32[8,1024]{1,0:T(8,128)} %get-tuple-element.12.affine_ref, bf16[4,3,2,256,256]{4,3,2,1,0:T(8,128)(2,1)} %all_to_all.10.w0_ref, ...), custom_call_target="tpu_custom_call" | custom-call | flops 2415919104 | bytes 8388608 | tf_op jit(solution)/shard_map/pallas_call | solution.py:181
  (20 shorter events, 0.7 us)
Async XLA Ops:
  69.8 7.7 %collective-permute-start.2 = (bf16[2,256,256]{2,1,0:T(8,128)(2,1)S(1)}, bf16[2,256,256]{2,1,0:T(8,128)(2,1)S(1)}, u32[]{:S(2)}, u32[]{:S(2)}) collective-permute-start(bf16[2,256,256]{2,1,0:T(8,128)(2,1)S(1)} %bitcast.31), channel_id=1, source_target_pairs={{0,256},{256,0},{1,257},{257,1},{2,258},{258,2},{3,259},{259,3},{4... | collective-permute-start | bytes 786440 | tf_op jit(solution)/shard_map/ppermute | solution.py:24
  77.6 10.0 %collective-permute-start.3 = (bf16[2,2,256,256]{3,2,1,0:T(8,128)(2,1)S(1)}, bf16[2,2,256,256]{3,2,1,0:T(8,128)(2,1)S(1)}, u32[]{:S(2)}, u32[]{:S(2)}) collective-permute-start(bf16[2,2,256,256]{3,2,1,0:T(8,128)(2,1)S(1)} %pad_maximum_fusion.1), channel_id=1, source_target_pairs={{0,8},{8,0},{1,9},{9,1},{2,10},{10,2},{3,11},{11,3},{4,12},{12,4},... | collective-permute-start | bytes 1572872 | tf_op jit(solution)/shard_map/ppermute | solution.py:24
  120.4 81.8 %collective-permute-start.4 = (bf16[4,3,2,256,256]{4,3,2,1,0:T(8,128)(2,1)}, bf16[4,3,2,256,256]{4,3,2,1,0:T(8,128)(2,1)}, u32[]{:S(2)}, u32[]{:S(2)}) collective-permute-start(bf16[4,3,2,256,256]{4,3,2,1,0:T(8,128)(2,1)} %all_to_all.10.w0_ref), channel_id=1, source_target_pairs={{0,1},{1,0},{2,3},{3,2},{4,5},{5,4},{6,7},{7,6},{8,9},{9,8},{10,11... | collective-permute-start | bytes 9437192 | tf_op jit(solution)/shard_map/ppermute | solution.py:24
  155.8 38.0 %copy-start = (bf16[4,3,256,256]{3,2,1,0:T(8,128)(2,1)}, bf16[4,3,256,256]{3,2,1,0:T(8,128)(2,1)S(1)}, u32[]{:S(2)}) copy-start(bf16[4,3,256,256]{3,2,1,0:T(8,128)(2,1)S(1)} %all_to_all.11.w0_ref.refs_0_) | copy-start | bytes 4718596
  155.8 38.0 %collective-permute-start.1 = (bf16[4,3,256,256]{3,2,1,0:T(8,128)(2,1)S(1)}, bf16[4,3,256,256]{3,2,1,0:T(8,128)(2,1)S(1)}, u32[]{:S(2)}, u32[]{:S(2)}) collective-permute-start(bf16[4,3,256,256]{3,2,1,0:T(8,128)(2,1)S(1)} %all_to_all.11.w0_ref.refs_0_), channel_id=1, source_target_pairs={{0,1},{1,0},{2,3},{3,2},{4,5},{5,4},{6,7},{7,6},{8,9},{9,8},{10,11... | collective-permute-start | bytes 4718600 | tf_op jit(solution)/shard_map/ppermute | solution.py:24
  158.9 15.5 %collective-permute-start.6 = (bf16[4,256,256]{2,1,0:T(8,128)(2,1)S(1)}, bf16[4,256,256]{2,1,0:T(8,128)(2,1)}, u32[]{:S(2)}, u32[]{:S(2)}) collective-permute-start(bf16[4,256,256]{2,1,0:T(8,128)(2,1)S(1)} %slice_bitcast_fusion), channel_id=1, source_target_pairs={{0,8},{8,0},{1,9},{9,1},{2,10},{10,2},{3,11},{11,3},{4,12},{12,4},... | collective-permute-start | bytes 1572872 | tf_op jit(solution)/shard_map/ppermute | solution.py:24
  162.3 25.7 %collective-permute-start.5 = (bf16[4,256,256]{2,1,0:T(8,128)(2,1)S(1)}, bf16[4,256,256]{2,1,0:T(8,128)(2,1)}, u32[]{:S(2)}, u32[]{:S(2)}) collective-permute-start(bf16[4,256,256]{2,1,0:T(8,128)(2,1)S(1)} %slice_bitcast_fusion), channel_id=1, source_target_pairs={{0,256},{256,0},{1,257},{257,1},{2,258},{258,2},{3,259},{259,3},{4... | collective-permute-start | bytes 1572872 | tf_op jit(solution)/shard_map/ppermute | solution.py:24
  174.4 15.5 %collective-permute-start.7 = (bf16[4,256,256]{2,1,0:T(8,128)(2,1)}, bf16[4,256,256]{2,1,0:T(8,128)(2,1)}, u32[]{:S(2)}, u32[]{:S(2)}) collective-permute-start(bf16[4,256,256]{2,1,0:T(8,128)(2,1)} %collective-permute-done.6.refs_2_), channel_id=1, source_target_pairs={{0,256},{256,0},{1,257},{257,1},{2,258},{258,2},{3,259},{259,3},{4... | collective-permute-start | bytes 1572872 | tf_op jit(solution)/shard_map/ppermute | solution.py:24
  178.8 5.3 %collective-permute-start = (bf16[32,2048]{1,0:T(8,128)(2,1)S(1)}, bf16[32,2048]{1,0:T(8,128)(2,1)S(1)}, u32[]{:S(2)}, u32[]{:S(2)}) collective-permute-start(bf16[32,2048]{1,0:T(8,128)(2,1)S(1)} %slice_bitcast_fusion.1), channel_id=1, source_target_pairs={{0,8},{8,16},{16,24},{24,32},{32,40},{40,48},{48,56},{56,64},{64,7... | collective-permute-start | bytes 393224 | tf_op jit(solution)/shard_map/ppermute | solution.py:212
  184.1 9.7 %copy-start.2 = (bf16[32,2048]{1,0:T(8,128)(2,1)}, bf16[32,2048]{1,0:T(8,128)(2,1)S(1)}, u32[]{:S(2)}) copy-start(bf16[32,2048]{1,0:T(8,128)(2,1)S(1)} %collective-permute-done.halo_ref) | copy-start | bytes 393220
  184.1 18.1 %collective-permute-start.9 = (bf16[4,256,256]{2,1,0:T(8,128)(2,1)}, bf16[4,256,256]{2,1,0:T(8,128)(2,1)}, u32[]{:S(2)}, u32[]{:S(2)}) collective-permute-start(bf16[4,256,256]{2,1,0:T(8,128)(2,1)} %collective-permute-done.6.refs_2_), channel_id=1, source_target_pairs={{0,1},{1,0},{2,3},{3,2},{4,5},{5,4},{6,7},{7,6},{8,9},{9,8},{10,11... | collective-permute-start | bytes 1572872 | tf_op jit(solution)/shard_map/ppermute | solution.py:24
  188.0 14.2 %collective-permute-start.8 = (bf16[4,256,256]{2,1,0:T(8,128)(2,1)}, bf16[4,256,256]{2,1,0:T(8,128)(2,1)}, u32[]{:S(2)}, u32[]{:S(2)}) collective-permute-start(bf16[4,256,256]{2,1,0:T(8,128)(2,1)} %collective-permute-done.5.refs_1_), channel_id=1, source_target_pairs={{0,1},{1,0},{2,3},{3,2},{4,5},{5,4},{6,7},{7,6},{8,9},{9,8},{10,11... | collective-permute-start | bytes 1572872 | tf_op jit(solution)/shard_map/ppermute | solution.py:24
  190.0 12.2 %collective-permute-start.10 = (bf16[4,256,256]{2,1,0:T(8,128)(2,1)}, bf16[4,256,256]{2,1,0:T(8,128)(2,1)}, u32[]{:S(2)}, u32[]{:S(2)}) collective-permute-start(bf16[4,256,256]{2,1,0:T(8,128)(2,1)} %collective-permute-done.7.refs_3_), channel_id=1, source_target_pairs={{0,1},{1,0},{2,3},{3,2},{4,5},{5,4},{6,7},{7,6},{8,9},{9,8},{10,11... | collective-permute-start | bytes 1572872 | tf_op jit(solution)/shard_map/ppermute | solution.py:24
  193.8 1.1 copy-start.1

commit v2 on v1

--- a/solution.py
+++ b/solution.py
@@ -80,10 +80,11 @@
 
 
 def first(
-    where_ref, halo_ref, tok_ref, cw_ref, gain_ref, bias_ref, w0_ref, w1_ref, conv_ref, stats_ref, tok_out, cw_out, affine_out,
+    where_ref, halo_ref, tok_ref, cw_ref, gain_ref, bias_ref, w0_ref, w1_ref, side0_ref, side1_ref,
+    conv_ref, stats_ref, tok_out, cw_out, affine_out,
     tok, cw, w, shifted, taps, raw, affine, sems,
 ):
-    blocks = w.shape[1]
+    blocks = w.shape[2]
     rows, deep = tok_ref.shape[0], tok.shape[1] // (2 * blocks)
     loads = [pltpu.make_async_copy(cw_ref, taps, sems.at[0])]
     for at in range(2 * blocks):
@@ -91,10 +92,11 @@
         loads.append(pltpu.make_async_copy(halo_ref.at[:, there], tok.at[pl.ds(0, HALO), here], sems.at[8 + 2 * at]))
         loads.append(pltpu.make_async_copy(tok_ref.at[:, there], tok.at[pl.ds(HALO, rows), here], sems.at[9 + 2 * at]))
     for m, r in enumerate((w0_ref, w1_ref)):
-        loads.append(pltpu.make_async_copy(r.at[:, pl.ds(0, 2)], w.at[m], sems.at[1 + m]))
+        loads.append(pltpu.make_async_copy(r.at[:, pl.ds(0, 2)], w.at[0, m], sems.at[1 + m]))
+    later = [pltpu.make_async_copy(r, w.at[1, m], sems.at[8 + 4 * blocks + m]) for m, r in enumerate((side0_ref, side1_ref))]
     loads.append(pltpu.make_async_copy(gain_ref, raw.at[pl.ds(0, 1)], sems.at[5]))
     loads.append(pltpu.make_async_copy(bias_ref, raw.at[pl.ds(8, 1)], sems.at[6]))
-    for load in loads:
+    for load in loads + later:
         load.start()
     loads[0].wait()
     loads[-2].wait()
@@ -113,7 +115,12 @@
     ]
     for store in stores:
         store.start()
-    convolve(True, tok, cw.at[pl.ds(0, 1)], joined(w, blocks, 0), joined(w, blocks, 1), conv_ref, stats_ref, shifted)
+    for load in later:
+        load.wait()
+    for q in range(2):
+        piece = w.at[q]
+        value, gate = joined(piece, blocks, 0), joined(piece, blocks, 1)
+        convolve(q == 0, tok, cw.at[pl.ds(q, 1)], value, gate, conv_ref.at[q], stats_ref, shifted)
     for store in stores:
         store.wait()
 
@@ -137,7 +144,7 @@
 
     early = [load(tok_ref, tok), load(cw_ref, cw)]
     pieces = [[load(r.at[:, i], w.at[i, m]) for m, r in enumerate((w0_ref, w1_ref))] for i in range(count)]
-    middle = [load(first_ref, conv.at[0]), load(stats_ref, stats), load(affine_ref, affine)]
+    middle = [load(first_ref, conv.at[pl.ds(0, 2)]), load(stats_ref, stats), load(affine_ref, affine)]
     late = []
     for i, r in enumerate(o_refs):
         m, q = i // len(QUARTERS), i % len(QUARTERS)
@@ -153,7 +160,7 @@
             wait(pieces[i])
         piece = w.at[i]
         value, gate = joined(piece, blocks, 0), joined(piece, blocks, 1)
-        convolve(i == 0, tok, cw.at[pl.ds(1 + i, 1)], value, gate, conv.at[1 + i], more, shifted)
+        convolve(i == 0, tok, cw.at[pl.ds(2 + i, 1)], value, gate, conv.at[2 + i], more, shifted)
     wait(middle)
     mean = jnp.sum(stats[0] + more[0], axis=1, keepdims=True) / channels
     meansq = jnp.sum(stats[1] + more[1], axis=1, keepdims=True) / channels
@@ -205,13 +212,15 @@
     own = own.reshape(3, -1, mine.shape[-1])
 
     vg = own[:2]
+    own0 = exchanged(copies(own, "x"), "x")
     vg_side = swapped(vg, "side")
-    own0 = exchanged(copies(own, "x"), "x")
-    vg_zl = swapped(jnp.stack([vg, vg_side]), "zl")
+    vg_zl = swapped(vg, "zl")
     last = rows[length - HALO :]
     halo = lax.ppermute(last, ("zh", "zl"), [(i, i + 1) for i in range(positions - 1)])
-    rest = jnp.concatenate([vg_side[None], vg_zl], axis=0)
-    rest0 = exchanged(copies(rest, "x"), "x")
+    side0 = exchanged(copies(vg_side, "x"), "x")
+    vg_both = swapped(vg_zl, "side")
+    rest0 = exchanged(copies(jnp.stack([vg_zl, vg_both]), "x"), "x")
+    side1 = swapped(side0, "core")
     o00 = own0[:, 2]
     o10 = swapped(o00, "side")
     o01 = swapped(o00, "zl")
@@ -230,18 +239,18 @@
     shifted = vmem((8, length + HALO, part), jnp.float32)
     flops = 2 * length * depth * channels // 2
     conv_a, stats_a, tok_ready, cw_ready, affine = kernel(
-        first, [SMEM] + [HBM] * 5 + [ANY] * 2,
-        [(shape((length, part), jnp.bfloat16), VMEM), stats, (shape(*tok), HBM), (shape(*cw), HBM),
+        first, [SMEM] + [HBM] * 5 + [ANY] * 4,
+        [(shape((2, length, part), jnp.bfloat16), VMEM), stats, (shape(*tok), HBM), (shape(*cw), HBM),
          (shape((8, channels), jnp.float32), HBM)],
-        [vmem(*tok), vmem(*cw), vmem((2, blocks, 2, part, deep), jnp.bfloat16), shifted,
+        [vmem(*tok), vmem(*cw), vmem((2, 2, blocks, 2, part, deep), jnp.bfloat16), shifted,
          vmem((taps, channels), jnp.bfloat16), vmem((16, channels), jnp.float32),
-         vmem((8, channels), jnp.float32), dma((8 + 4 * blocks,))],
-        flops, 56, where, halo, rows, conv_weight, norm_gain[None], norm_bias[None], own0, own1,
+         vmem((8, channels), jnp.float32), dma((10 + 4 * blocks,))],
+        flops, 56, where, halo, rows, conv_weight, norm_gain[None], norm_bias[None], own0, own1, side0, side1,
     )
     (mixed,) = kernel(
         remaining, [SMEM, HBM, HBM, HBM, ANY, ANY, HBM, HBM] + [ANY] * 8,
         [(shape((length, depth), jnp.bfloat16), HBM)],
-        [vmem(*tok), vmem(*cw), vmem((3, 2, blocks, 2, part, deep), jnp.bfloat16), shifted,
+        [vmem(*tok), vmem(*cw), vmem((2, 2, blocks, 2, part, deep), jnp.bfloat16), shifted,
          vmem((4, length, part), jnp.bfloat16), vmem((length, channels), jnp.bfloat16),
          vmem((2, length, LANES), jnp.float32), vmem((2, length, LANES), jnp.float32),
          vmem((8, channels), jnp.float32), vmem((2, 4, blocks, part, deep), jnp.bfloat16),

time: 216 us -> 224 us (1.037)
  blocking collectives: 124 us -> 69 us
  waiting for transfers between devices: 20.9 us -> 52.7 us
  starting transfers between devices: 45.2 us -> 72.9 us
  local copies, waits for them, and re-layouts: 2.62 us -> 6.66 us
    all_to_all x2 -> x0, blocking collectives: 55.4 us -> none  [exchanged(): return lax.all_to_all(blocks, axis, 0, 0)]
    ppermute x10 -> x12, starting transfers between devices: 41.8 us -> 58.7 us  [swapped(): return lax.ppermute(array, axis, [(0, 1), (1, 0)])]
    all_to_all x0 -> x3, waiting for transfers between devices: none -> 15.5 us  [exchanged(): return lax.all_to_all(blocks, axis, 0, 0)]
    all_to_all x0 -> x3, starting transfers between devices: none -> 12.3 us  [exchanged(): return lax.all_to_all(blocks, axis, 0, 0)]
    ppermute x1, waiting for transfers between devices: 1.92 us -> 11.2 us  [per_device(): lax.ppermute(last, ('zh', 'zl'), [(i, i + 1) for i in range(positions - 1)])]
    ppermute x10 -> x12, waiting for transfers between devices: 19 us -> 26 us  [swapped(): return lax.ppermute(array, axis, [(0, 1), (1, 0)])]
    broadcast_in_dim x2 -> x3, local copies, waits for them, and re-layouts: 0.46 us -> 3.95 us  [copies(): return jnp.broadcast_to(block, (lax.axis_size(axis), *block.shape))]
  transfers between devices with their start and end apart: 11 -> 16, of which waited for: 4 -> 7; matrix products, arithmetic and copies ran while one was open for 1% -> 1% of each run, Pallas kernels for 3% -> 4%
where the time goes in v2:
time: 224 us; the launch traced here: 223 us
  starting transfers between devices  72.9 us (33%)
  blocking collectives  69 us (31%)
  waiting for transfers between devices  52.7 us (24%)
  Pallas kernels  20.3 us (9%)
  local copies, waits for them, and re-layouts  6.66 us (3%)
    all_gather x1, blocking collectives, per_device(): far = lax.all_gather(mine, 'zh', axis=0, tiled=True)  69 us
    ppermute x12, starting transfers between devices, swapped(): return lax.ppermute(array, axis, [(0, 1), (1, 0)])  58.7 us
    ppermute x12, waiting for transfers between devices, swapped(): return lax.ppermute(array, axis, [(0, 1), (1, 0)])  26 us
    pallas_call x2, Pallas kernels, kernel(): pl.pallas_call(function, out_shape=[o[0] for o in outs], in_specs=specs,...  20.3 us
    all_to_all x3, waiting for transfers between devices, exchanged(): return lax.all_to_all(blocks, axis, 0, 0)  15.5 us
    all_to_all x3, starting transfers between devices, exchanged(): return lax.all_to_all(blocks, axis, 0, 0)  12.3 us
    ppermute x1, waiting for transfers between devices, per_device(): lax.ppermute(last, ('zh', 'zl'), [(i, i + 1) for i in range(positions - 1)])  11.2 us
  transfers between devices with their start and end apart: 16, of which 7 were waited for; matrix products, arithmetic and copies ran while one was open for 1% of the time, Pallas kernels for 4%

profile of v2, /device:TPU:33, one launch (start us, length us, event | category | flops | bytes accessed | tf_op | source)
XLA Modules:
  0.0 223.4 jit_solution(17693303165284103266)
XLA Ops:
  0.7 69.0 %all_gather.3 = bf16[48,16,256]{2,1,0:T(8,128)(2,1)S(1)} all-gather(bf16[3,16,256]{2,1,0:T(8,128)(2,1)S(1)} %fusion.1), channel_id=1, replica_groups=mesh['pair'=1,'side'=2,'zh'=16,'zl'=2,'x'=4,'core'=2] {'zh'}, dimensions={0}, use_global_device_ids=true | all-gather | bytes 417792 | tf_op jit(solution)/shard_map/all_gather | solution.py:210
  69.8 4.0 %collective-permute-start.2 = (bf16[2,256,256]{2,1,0:T(8,128)(2,1)S(1)}, bf16[2,256,256]{2,1,0:T(8,128)(2,1)S(1)}, u32[]{:S(2)}, u32[]{:S(2)}) collective-permute-start(bf16[2,256,256]{2,1,0:T(8,128)(2,1)S(1)} %bitcast.31), channel_id=1, source_target_pairs={{0,256},{256,0},{1,257},{257,1},{2,258},{258,2},{3,259},{259,3},{4... | collective-permute-start | bytes 786440 | tf_op jit(solution)/shard_map/ppermute | solution.py:24
  73.8 3.7 %collective-permute-done.2 = bf16[2,256,256]{2,1,0:T(8,128)(2,1)S(1)} collective-permute-done((bf16[2,256,256]{2,1,0:T(8,128)(2,1)S(1)}, bf16[2,256,256]{2,1,0:T(8,128)(2,1)S(1)}, u32[]{:S(2)}, u32[]{:S(2)}) %collective-permute-start.2) | collective-permute-done | bytes 262176 | tf_op jit(solution)/shard_map/ppermute | solution.py:24
  78.6 4.3 %all-to-all-start.1 = ((bf16[4,2,256,256]{3,2,1,0:T(8,128)(2,1)}), bf16[4,2,256,256]{3,2,1,0:T(8,128)(2,1)}, u32[]{:S(2)}, u32[]{:S(2)}) async-start(bf16[4,2,256,256]{3,2,1,0:T(8,128)(2,1)} %broadcast_in_dim.21), calls=%async_computation.1 | async-start | bytes 2097152 | tf_op jit(solution)/shard_map/all_to_all | solution.py:20
  82.9 3.4 %collective-permute-start.4 = (bf16[2,256,256]{2,1,0:T(8,128)(2,1)S(1)}, bf16[2,256,256]{2,1,0:T(8,128)(2,1)S(1)}, u32[]{:S(2)}, u32[]{:S(2)}) collective-permute-start(bf16[2,256,256]{2,1,0:T(8,128)(2,1)S(1)} %bitcast.32), channel_id=1, source_target_pairs={{0,8},{8,0},{1,9},{9,1},{2,10},{10,2},{3,11},{11,3},{4,12},{12,4},... | collective-permute-start | bytes 786440 | tf_op jit(solution)/shard_map/ppermute | solution.py:24
  86.3 3.8 %collective-permute-done.4 = bf16[2,256,256]{2,1,0:T(8,128)(2,1)S(1)} collective-permute-done((bf16[2,256,256]{2,1,0:T(8,128)(2,1)S(1)}, bf16[2,256,256]{2,1,0:T(8,128)(2,1)S(1)}, u32[]{:S(2)}, u32[]{:S(2)}) %collective-permute-start.4) | collective-permute-done | bytes 262176 | tf_op jit(solution)/shard_map/ppermute | solution.py:24
  90.1 3.4 %collective-permute-start.5 = (bf16[2,256,256]{2,1,0:T(8,128)(2,1)S(1)}, bf16[2,256,256]{2,1,0:T(8,128)(2,1)S(1)}, u32[]{:S(2)}, u32[]{:S(2)}) collective-permute-start(bf16[2,256,256]{2,1,0:T(8,128)(2,1)S(1)} %collective-permute-done.4), channel_id=1, source_target_pairs={{0,256},{256,0},{1,257},{257,1},{2,258},{258,2},{3,259},{259,3},{4... | collective-permute-start | bytes 786440 | tf_op jit(solution)/shard_map/ppermute | solution.py:24
  93.5 4.1 %collective-permute-done.5 = bf16[2,256,256]{2,1,0:T(8,128)(2,1)S(1)} collective-permute-done((bf16[2,256,256]{2,1,0:T(8,128)(2,1)S(1)}, bf16[2,256,256]{2,1,0:T(8,128)(2,1)S(1)}, u32[]{:S(2)}, u32[]{:S(2)}) %collective-permute-start.5) | collective-permute-done | bytes 262176 | tf_op jit(solution)/shard_map/ppermute | solution.py:24
  99.2 4.3 %all-to-all-start.2 = ((bf16[4,2,2,256,256]{4,3,2,1,0:T(8,128)(2,1)}), bf16[4,2,2,256,256]{4,3,2,1,0:T(8,128)(2,1)S(1)}, u32[]{:S(2)}, u32[]{:S(2)}) async-start(bf16[4,2,2,256,256]{4,3,2,1,0:T(8,128)(2,1)} %broadcast_in_dim.22), calls=%async_computation.2 | async-start | bytes 4194304 | tf_op jit(solution)/shard_map/all_to_all | solution.py:20
  103.5 15.4 %all-to-all-done.2.w0_ref = bf16[4,2,2,256,256]{4,3,2,1,0:T(8,128)(2,1)S(1)} async-done(((bf16[4,2,2,256,256]{4,3,2,1,0:T(8,128)(2,1)}), bf16[4,2,2,256,256]{4,3,2,1,0:T(8,128)(2,1)S(1)}, u32[]{:S(2)}, u32[]{:S(2)}) %all-to-all-start.2) | async-done | bytes 2097184 | tf_op jit(solution)/shard_map/all_to_all | solution.py:20
  120.8 3.7 %all-to-all-start = ((bf16[4,3,256,256]{3,2,1,0:T(8,128)(2,1)}), bf16[4,3,256,256]{3,2,1,0:T(8,128)(2,1)S(1)}, u32[]{:S(2)}, u32[]{:S(2)}) async-start(bf16[4,3,256,256]{3,2,1,0:T(8,128)(2,1)} %broadcast_in_dim.20), calls=%async_computation | async-start | bytes 3145728 | tf_op jit(solution)/shard_map/all_to_all | solution.py:20
  124.5 15.3 %collective-permute-start.6 = (bf16[4,2,2,256,256]{4,3,2,1,0:T(8,128)(2,1)}, bf16[4,2,2,256,256]{4,3,2,1,0:T(8,128)(2,1)}, u32[]{:S(2)}, u32[]{:S(2)}) collective-permute-start(bf16[4,2,2,256,256]{4,3,2,1,0:T(8,128)(2,1)} %copy-done.1), channel_id=1, source_target_pairs={{0,1},{1,0},{2,3},{3,2},{4,5},{5,4},{6,7},{7,6},{8,9},{9,8},{10,11... | collective-permute-start | bytes 6291464 | tf_op jit(solution)/shard_map/ppermute | solution.py:24
  141.8 11.6 %collective-permute-start.1 = (bf16[4,3,256,256]{3,2,1,0:T(8,128)(2,1)S(1)}, bf16[4,3,256,256]{3,2,1,0:T(8,128)(2,1)S(1)}, u32[]{:S(2)}, u32[]{:S(2)}) collective-permute-start(bf16[4,3,256,256]{3,2,1,0:T(8,128)(2,1)S(1)} %all-to-all-done.w0_ref.refs_0_), channel_id=1, source_target_pairs={{0,1},{1,0},{2,3},{3,2},{4,5},{5,4},{6,7},{7,6},{8,9},{9,8},{10,11... | collective-permute-start | bytes 4718600 | tf_op jit(solution)/shard_map/ppermute | solution.py:24
  153.4 3.4 %collective-permute-start.8 = (bf16[4,256,256]{2,1,0:T(8,128)(2,1)S(1)}, bf16[4,256,256]{2,1,0:T(8,128)(2,1)}, u32[]{:S(2)}, u32[]{:S(2)}) collective-permute-start(bf16[4,256,256]{2,1,0:T(8,128)(2,1)S(1)} %slice_bitcast_fusion), channel_id=1, source_target_pairs={{0,8},{8,0},{1,9},{9,1},{2,10},{10,2},{3,11},{11,3},{4,12},{12,4},... | collective-permute-start | bytes 1572872 | tf_op jit(solution)/shard_map/ppermute | solution.py:24
  157.8 2.0 collective-permute-start
  159.7 11.2 %collective-permute-done.halo_ref = bf16[32,2048]{1,0:T(8,128)(2,1)S(1)} collective-permute-done((bf16[32,2048]{1,0:T(8,128)(2,1)S(1)}, bf16[32,2048]{1,0:T(8,128)(2,1)S(1)}, u32[]{:S(2)}, u32[]{:S(2)}) %collective-permute-start) | collective-permute-done | bytes 131104 | tf_op jit(solution)/shard_map/ppermute | solution.py:219
  170.9 3.8 %collective-permute-start.7 = (bf16[4,256,256]{2,1,0:T(8,128)(2,1)S(1)}, bf16[4,256,256]{2,1,0:T(8,128)(2,1)}, u32[]{:S(2)}, u32[]{:S(2)}) collective-permute-start(bf16[4,256,256]{2,1,0:T(8,128)(2,1)S(1)} %slice_bitcast_fusion), channel_id=1, source_target_pairs={{0,256},{256,0},{1,257},{257,1},{2,258},{258,2},{3,259},{259,3},{4... | collective-permute-start | bytes 1572872 | tf_op jit(solution)/shard_map/ppermute | solution.py:24
  176.7 9.5 %collective-permute-done.7.refs_1_ = bf16[4,256,256]{2,1,0:T(8,128)(2,1)} collective-permute-done((bf16[4,256,256]{2,1,0:T(8,128)(2,1)S(1)}, bf16[4,256,256]{2,1,0:T(8,128)(2,1)}, u32[]{:S(2)}, u32[]{:S(2)}) %collective-permute-start.7) | collective-permute-done | bytes 524320 | tf_op jit(solution)/shard_map/ppermute | solution.py:24
  186.2 4.4 %collective-permute-start.11 = (bf16[4,256,256]{2,1,0:T(8,128)(2,1)}, bf16[4,256,256]{2,1,0:T(8,128)(2,1)}, u32[]{:S(2)}, u32[]{:S(2)}) collective-permute-start(bf16[4,256,256]{2,1,0:T(8,128)(2,1)} %collective-permute-done.8.refs_2_), channel_id=1, source_target_pairs={{0,1},{1,0},{2,3},{3,2},{4,5},{5,4},{6,7},{7,6},{8,9},{9,8},{10,11... | collective-permute-start | bytes 1572872 | tf_op jit(solution)/shard_map/ppermute | solution.py:24
  190.7 2.0 collective-permute-start.10
  192.6 4.8 %collective-permute-done.9.refs_3_ = bf16[4,256,256]{2,1,0:T(8,128)(2,1)} collective-permute-done((bf16[4,256,256]{2,1,0:T(8,128)(2,1)}, bf16[4,256,256]{2,1,0:T(8,128)(2,1)}, u32[]{:S(2)}, u32[]{:S(2)}) %collective-permute-start.9) | collective-permute-done | bytes 524320 | tf_op jit(solution)/shard_map/ppermute | solution.py:24
  197.5 3.6 %collective-permute-start.12 = (bf16[4,256,256]{2,1,0:T(8,128)(2,1)}, bf16[4,256,256]{2,1,0:T(8,128)(2,1)}, u32[]{:S(2)}, u32[]{:S(2)}) collective-permute-start(bf16[4,256,256]{2,1,0:T(8,128)(2,1)} %collective-permute-done.9.refs_3_), channel_id=1, source_target_pairs={{0,1},{1,0},{2,3},{3,2},{4,5},{5,4},{6,7},{7,6},{8,9},{9,8},{10,11... | collective-permute-start | bytes 1572872 | tf_op jit(solution)/shard_map/ppermute | solution.py:24
  202.9 9.5 %shard_map.73 = (bf16[2,384,256]{2,1,0:T(8,128)(2,1)}, f32[2,384,128]{2,1,0:T(8,128)}, bf16[416,2048]{1,0:T(8,128)(2,1)}, f32[4,31,256]{2,1,0:T(8,128)}, f32[8,1024]{1,0:T(8,128)}) custom-call(s32[3]{0:T(128)} %pad_add_fusion.where_ref, bf16[32,2048]{1,0:T(8,128)(2,1)} %copy-done.3, bf16[384,2048]{1,0:T(8,128)(2,1)} %bitcast.29, bf16[31,1024]{1,0:T(8,128)(2,1)} %cw_ref.1, ...), custom_call_target="tpu_custom_call" | custom-call | flops 805306368 | bytes 8388608 | tf_op jit(solution)/shard_map/pallas_call | solution.py:188
  212.4 10.8 %shard_map.74 = bf16[384,2048]{1,0:T(8,128)(2,1)} custom-call(s32[3]{0:T(128)} %pad_add_fusion.where_ref, bf16[416,2048]{1,0:T(8,128)(2,1)} %get-tuple-element.10.tok_ref, f32[4,31,256]{2,1,0:T(8,128)} %get-tuple-element.11.cw_ref, f32[8,1024]{1,0:T(8,128)} %get-tuple-element.12.affine_ref, bf16[4,2,2,256,256]{4,3,2,1,0:T(8,128)(2,1)} %copy-done.1, ...), custom_call_target="tpu_custom_call" | custom-call | flops 2415919104 | bytes 8388608 | tf_op jit(solution)/shard_map/pallas_call | solution.py:188
  (30 shorter events, 12.0 us)
Async XLA Ops:
  69.8 7.7 %collective-permute-start.2 = (bf16[2,256,256]{2,1,0:T(8,128)(2,1)S(1)}, bf16[2,256,256]{2,1,0:T(8,128)(2,1)S(1)}, u32[]{:S(2)}, u32[]{:S(2)}) collective-permute-start(bf16[2,256,256]{2,1,0:T(8,128)(2,1)S(1)} %bitcast.31), channel_id=1, source_target_pairs={{0,256},{256,0},{1,257},{257,1},{2,258},{258,2},{3,259},{259,3},{4... | collective-permute-start | bytes 786440 | tf_op jit(solution)/shard_map/ppermute | solution.py:24
  78.6 19.1 %all-to-all-start.1 = ((bf16[4,2,256,256]{3,2,1,0:T(8,128)(2,1)}), bf16[4,2,256,256]{3,2,1,0:T(8,128)(2,1)}, u32[]{:S(2)}, u32[]{:S(2)}) async-start(bf16[4,2,256,256]{3,2,1,0:T(8,128)(2,1)} %broadcast_in_dim.21), calls=%async_computation.1 | async-start | bytes 2097152 | tf_op jit(solution)/shard_map/all_to_all | solution.py:20
  82.9 7.1 %collective-permute-start.4 = (bf16[2,256,256]{2,1,0:T(8,128)(2,1)S(1)}, bf16[2,256,256]{2,1,0:T(8,128)(2,1)S(1)}, u32[]{:S(2)}, u32[]{:S(2)}) collective-permute-start(bf16[2,256,256]{2,1,0:T(8,128)(2,1)S(1)} %bitcast.32), channel_id=1, source_target_pairs={{0,8},{8,0},{1,9},{9,1},{2,10},{10,2},{3,11},{11,3},{4,12},{12,4},... | collective-permute-start | bytes 786440 | tf_op jit(solution)/shard_map/ppermute | solution.py:24
  90.1 7.5 %collective-permute-start.5 = (bf16[2,256,256]{2,1,0:T(8,128)(2,1)S(1)}, bf16[2,256,256]{2,1,0:T(8,128)(2,1)S(1)}, u32[]{:S(2)}, u32[]{:S(2)}) collective-permute-start(bf16[2,256,256]{2,1,0:T(8,128)(2,1)S(1)} %collective-permute-done.4), channel_id=1, source_target_pairs={{0,256},{256,0},{1,257},{257,1},{2,258},{258,2},{3,259},{259,3},{4... | collective-permute-start | bytes 786440 | tf_op jit(solution)/shard_map/ppermute | solution.py:24
  99.2 19.7 %all-to-all-start.2 = ((bf16[4,2,2,256,256]{4,3,2,1,0:T(8,128)(2,1)}), bf16[4,2,2,256,256]{4,3,2,1,0:T(8,128)(2,1)S(1)}, u32[]{:S(2)}, u32[]{:S(2)}) async-start(bf16[4,2,2,256,256]{4,3,2,1,0:T(8,128)(2,1)} %broadcast_in_dim.22), calls=%async_computation.2 | async-start | bytes 4194304 | tf_op jit(solution)/shard_map/all_to_all | solution.py:20
  119.0 1.8 copy-start.1
  120.8 21.0 %all-to-all-start = ((bf16[4,3,256,256]{3,2,1,0:T(8,128)(2,1)}), bf16[4,3,256,256]{3,2,1,0:T(8,128)(2,1)S(1)}, u32[]{:S(2)}, u32[]{:S(2)}) async-start(bf16[4,3,256,256]{3,2,1,0:T(8,128)(2,1)} %broadcast_in_dim.20), calls=%async_computation | async-start | bytes 3145728 | tf_op jit(solution)/shard_map/all_to_all | solution.py:20
  124.5 87.9 %collective-permute-start.6 = (bf16[4,2,2,256,256]{4,3,2,1,0:T(8,128)(2,1)}, bf16[4,2,2,256,256]{4,3,2,1,0:T(8,128)(2,1)}, u32[]{:S(2)}, u32[]{:S(2)}) collective-permute-start(bf16[4,2,2,256,256]{4,3,2,1,0:T(8,128)(2,1)} %copy-done.1), channel_id=1, source_target_pairs={{0,1},{1,0},{2,3},{3,2},{4,5},{5,4},{6,7},{7,6},{8,9},{9,8},{10,11... | collective-permute-start | bytes 6291464 | tf_op jit(solution)/shard_map/ppermute | solution.py:24
  139.8 50.9 %collective-permute-start.3 = (bf16[4,2,256,256]{3,2,1,0:T(8,128)(2,1)}, bf16[4,2,256,256]{3,2,1,0:T(8,128)(2,1)}, u32[]{:S(2)}, u32[]{:S(2)}) collective-permute-start(bf16[4,2,256,256]{3,2,1,0:T(8,128)(2,1)} %all-to-all-done.1.side0_ref), channel_id=1, source_target_pairs={{0,1},{1,0},{2,3},{3,2},{4,5},{5,4},{6,7},{7,6},{8,9},{9,8},{10,11... | collective-permute-start | bytes 3145736 | tf_op jit(solution)/shard_map/ppermute | solution.py:24
  141.8 59.9 %copy-start = (bf16[4,3,256,256]{3,2,1,0:T(8,128)(2,1)}, bf16[4,3,256,256]{3,2,1,0:T(8,128)(2,1)S(1)}, u32[]{:S(2)}) copy-start(bf16[4,3,256,256]{3,2,1,0:T(8,128)(2,1)S(1)} %all-to-all-done.w0_ref.refs_0_) | copy-start | bytes 4718596
  141.8 59.8 %collective-permute-start.1 = (bf16[4,3,256,256]{3,2,1,0:T(8,128)(2,1)S(1)}, bf16[4,3,256,256]{3,2,1,0:T(8,128)(2,1)S(1)}, u32[]{:S(2)}, u32[]{:S(2)}) collective-permute-start(bf16[4,3,256,256]{3,2,1,0:T(8,128)(2,1)S(1)} %all-to-all-done.w0_ref.refs_0_), channel_id=1, source_target_pairs={{0,1},{1,0},{2,3},{3,2},{4,5},{5,4},{6,7},{7,6},{8,9},{9,8},{10,11... | collective-permute-start | bytes 4718600 | tf_op jit(solution)/shard_map/ppermute | solution.py:24
  153.4 21.3 %collective-permute-start.8 = (bf16[4,256,256]{2,1,0:T(8,128)(2,1)S(1)}, bf16[4,256,256]{2,1,0:T(8,128)(2,1)}, u32[]{:S(2)}, u32[]{:S(2)}) collective-permute-start(bf16[4,256,256]{2,1,0:T(8,128)(2,1)S(1)} %slice_bitcast_fusion), channel_id=1, source_target_pairs={{0,8},{8,0},{1,9},{9,1},{2,10},{10,2},{3,11},{11,3},{4,12},{12,4},... | collective-permute-start | bytes 1572872 | tf_op jit(solution)/shard_map/ppermute | solution.py:24
  157.8 13.1 %collective-permute-start = (bf16[32,2048]{1,0:T(8,128)(2,1)S(1)}, bf16[32,2048]{1,0:T(8,128)(2,1)S(1)}, u32[]{:S(2)}, u32[]{:S(2)}) collective-permute-start(bf16[32,2048]{1,0:T(8,128)(2,1)S(1)} %slice_bitcast_fusion.1), channel_id=1, source_target_pairs={{0,8},{8,16},{16,24},{24,32},{32,40},{40,48},{48,56},{56,64},{64,7... | collective-permute-start | bytes 393224 | tf_op jit(solution)/shard_map/ppermute | solution.py:219
  170.9 30.7 %copy-start.3 = (bf16[32,2048]{1,0:T(8,128)(2,1)}, bf16[32,2048]{1,0:T(8,128)(2,1)S(1)}, u32[]{:S(2)}) copy-start(bf16[32,2048]{1,0:T(8,128)(2,1)S(1)} %collective-permute-done.halo_ref) | copy-start | bytes 393220
  170.9 15.3 %collective-permute-start.7 = (bf16[4,256,256]{2,1,0:T(8,128)(2,1)S(1)}, bf16[4,256,256]{2,1,0:T(8,128)(2,1)}, u32[]{:S(2)}, u32[]{:S(2)}) collective-permute-start(bf16[4,256,256]{2,1,0:T(8,128)(2,1)S(1)} %slice_bitcast_fusion), channel_id=1, source_target_pairs={{0,256},{256,0},{1,257},{257,1},{2,258},{258,2},{3,259},{259,3},{4... | collective-permute-start | bytes 1572872 | tf_op jit(solution)/shard_map/ppermute | solution.py:24
  174.7 22.7 %collective-permute-start.9 = (bf16[4,256,256]{2,1,0:T(8,128)(2,1)}, bf16[4,256,256]{2,1,0:T(8,128)(2,1)}, u32[]{:S(2)}, u32[]{:S(2)}) collective-permute-start(bf16[4,256,256]{2,1,0:T(8,128)(2,1)} %collective-permute-done.8.refs_2_), channel_id=1, source_target_pairs={{0,256},{256,0},{1,257},{257,1},{2,258},{258,2},{3,259},{259,3},{4... | collective-permute-start | bytes 1572872 | tf_op jit(solution)/shard_map/ppermute | solution.py:24
  186.2 26.1 %collective-permute-start.11 = (bf16[4,256,256]{2,1,0:T(8,128)(2,1)}, bf16[4,256,256]{2,1,0:T(8,128)(2,1)}, u32[]{:S(2)}, u32[]{:S(2)}) collective-permute-start(bf16[4,256,256]{2,1,0:T(8,128)(2,1)} %collective-permute-done.8.refs_2_), channel_id=1, source_target_pairs={{0,1},{1,0},{2,3},{3,2},{4,5},{5,4},{6,7},{7,6},{8,9},{9,8},{10,11... | collective-permute-start | bytes 1572872 | tf_op jit(solution)/shard_map/ppermute | solution.py:24
  190.7 21.7 %collective-permute-start.10 = (bf16[4,256,256]{2,1,0:T(8,128)(2,1)}, bf16[4,256,256]{2,1,0:T(8,128)(2,1)}, u32[]{:S(2)}, u32[]{:S(2)}) collective-permute-start(bf16[4,256,256]{2,1,0:T(8,128)(2,1)} %collective-permute-done.7.refs_1_), channel_id=1, source_target_pairs={{0,1},{1,0},{2,3},{3,2},{4,5},{5,4},{6,7},{7,6},{8,9},{9,8},{10,11... | collective-permute-start | bytes 1572872 | tf_op jit(solution)/shard_map/ppermute | solution.py:24
  197.5 14.9 %collective-permute-start.12 = (bf16[4,256,256]{2,1,0:T(8,128)(2,1)}, bf16[4,256,256]{2,1,0:T(8,128)(2,1)}, u32[]{:S(2)}, u32[]{:S(2)}) collective-permute-start(bf16[4,256,256]{2,1,0:T(8,128)(2,1)} %collective-permute-done.9.refs_3_), channel_id=1, source_target_pairs={{0,1},{1,0},{2,3},{3,2},{4,5},{5,4},{6,7},{7,6},{8,9},{9,8},{10,11... | collective-permute-start | bytes 1572872 | tf_op jit(solution)/shard_map/ppermute | solution.py:24
  201.6 1.2 copy-start.2

commit v3 on v1

--- a/solution.py
+++ b/solution.py
@@ -30,7 +30,7 @@
     return pl.ds(pl.multiple_of((2 * x + c) * deep, deep), deep)
 
 
-def chosen(array, where_ref, quarter, precision=None):
+def chosen(array, where_ref, quarter):
     side = where_ref[1] if quarter[0] == 0 else 1 - where_ref[1]
     parity = where_ref[2] if quarter[1] == 0 else 1 - where_ref[2]
     width = LANES // 8
@@ -40,7 +40,7 @@
     pick = source == (target // width) * (4 * width) + parity * (2 * width) + side * width + target % width
     pick = jnp.where(pick, 1.0, 0.0).astype(array.dtype)
     parts = [array[:, at : at + wide] for at in range(0, array.shape[1], wide)]
-    parts = [jnp.dot(p, pick, preferred_element_type=jnp.float32, precision=precision) for p in parts]
+    parts = [jnp.dot(p, pick, preferred_element_type=jnp.float32) for p in parts]
     return jnp.concatenate(parts, axis=1)
 
 
@@ -49,7 +49,7 @@
     taps = cw.shape[1]
     nt = (((1,), (1,)), ((), ()))
     value = lax.dot_general(tok[...], value, nt, preferred_element_type=jnp.float32)
-    gate = lax.dot_general(tok[...], gate, nt, preferred_element_type=jnp.float32)
+    gate = lax.dot_general(tok[...], gate(), nt, preferred_element_type=jnp.float32)
     glu = (value * jax.nn.sigmoid(gate)).astype(jnp.bfloat16).astype(jnp.float32)
     shifted[0] = glu
     for r in range(1, 8):
@@ -100,10 +100,14 @@
     loads[-2].wait()
     loads[-1].wait()
     pair = jnp.concatenate([raw[0:1], raw[8:9], jnp.zeros((6, raw.shape[1]), jnp.float32)], axis=0)
+    high = pair.astype(jnp.bfloat16).astype(jnp.float32)
+    middle = (pair - high).astype(jnp.bfloat16).astype(jnp.float32)
+    thirds = jnp.concatenate([high, middle, pair - high - middle, jnp.zeros_like(pair)], axis=0).astype(jnp.bfloat16)
     part = cw.shape[2]
     for i, quarter in enumerate(QUARTERS):
         cw[i] = chosen(taps[...], where_ref, quarter)
-        affine[:, i * part : (i + 1) * part] = chosen(pair, where_ref, quarter, lax.Precision.HIGHEST)
+        third = chosen(thirds, where_ref, quarter)
+        affine[:, i * part : (i + 1) * part] = third[0:8] + (third[8:16] + third[16:24])
     for load in loads[1:-2]:
         load.wait()
     stores = [
@@ -113,7 +117,7 @@
     ]
     for store in stores:
         store.start()
-    convolve(True, tok, cw.at[pl.ds(0, 1)], joined(w, blocks, 0), joined(w, blocks, 1), conv_ref, stats_ref, shifted)
+    convolve(True, tok, cw.at[pl.ds(0, 1)], joined(w, blocks, 0), lambda: joined(w, blocks, 1), conv_ref, stats_ref, shifted)
     for store in stores:
         store.wait()
 
@@ -136,15 +140,15 @@
             copy.wait()
 
     early = [load(tok_ref, tok), load(cw_ref, cw)]
-    pieces = [[load(r.at[:, i], w.at[i, m]) for m, r in enumerate((w0_ref, w1_ref))] for i in range(count)]
+    pieces = [[load(r.at[:, i], w.at[i, m]) for m, r in enumerate((w0_ref, w1_ref))] if i else [] for i in range(count)]
     middle = [load(first_ref, conv.at[0]), load(stats_ref, stats), load(affine_ref, affine)]
     late = []
     for i, r in enumerate(o_refs):
         m, q = i // len(QUARTERS), i % len(QUARTERS)
         late.append(load(r.at[:, 2] if q == 0 else r, o.at[m, q]))
-    start(early + pieces[0])
-    wait(early + pieces[0])
-    start(sum(pieces[1:], []) + middle)
+    head, tail = ([load(r.at[:, 0, k], w.at[0, m, :, k]) for m, r in enumerate((w0_ref, w1_ref))] for k in range(2))
+    start(early + head + tail)
+    wait(early + head)
     for i in range(count):
         if i == 1:
             wait(pieces[1])
@@ -152,7 +156,14 @@
         elif i > 1:
             wait(pieces[i])
         piece = w.at[i]
-        value, gate = joined(piece, blocks, 0), joined(piece, blocks, 1)
+
+        def gate(i=i, piece=piece):
+            if i == 0:
+                wait(tail)
+                start(sum(pieces[1:], []) + middle)
+            return joined(piece, blocks, 1)
+
+        value = joined(piece, blocks, 0)
         convolve(i == 0, tok, cw.at[pl.ds(1 + i, 1)], value, gate, conv.at[1 + i], more, shifted)
     wait(middle)
     mean = jnp.sum(stats[0] + more[0], axis=1, keepdims=True) / channels

time: 216 us -> 216 us (level)
  no operation moved by 1% of the time
where the time goes in v3:
time: 216 us; the launch traced here: 215 us
  blocking collectives  124 us (57%)
  starting transfers between devices  45.2 us (21%)
  waiting for transfers between devices  20.9 us (10%)
  Pallas kernels  20.2 us (9%)
  local copies, waits for them, and re-layouts  2.62 us (1%)
    all_gather x1, blocking collectives, per_device(): far = lax.all_gather(mine, 'zh', axis=0, tiled=True)  69 us
    all_to_all x2, blocking collectives, exchanged(): return lax.all_to_all(blocks, axis, 0, 0)  55.4 us
    ppermute x10, starting transfers between devices, swapped(): return lax.ppermute(array, axis, [(0, 1), (1, 0)])  41.8 us
    pallas_call x2, Pallas kernels, kernel(): pl.pallas_call(function, out_shape=[o[0] for o in outs], in_specs=specs,...  20.2 us
    ppermute x10, waiting for transfers between devices, swapped(): return lax.ppermute(array, axis, [(0, 1), (1, 0)])  19 us
  transfers between devices with their start and end apart: 11, of which 4 were waited for; matrix products, arithmetic and copies ran while one was open for 1% of the time, Pallas kernels for 3%

profile of v3, /device:TPU:33, one launch (start us, length us, event | category | flops | bytes accessed | tf_op | source)
XLA Modules:
  0.0 215.4 jit_solution(9129419005306297777)
XLA Ops:
  0.0 0.7 fusion.1
  0.7 69.0 %all_gather.3 = bf16[48,16,256]{2,1,0:T(8,128)(2,1)S(1)} all-gather(bf16[3,16,256]{2,1,0:T(8,128)(2,1)S(1)} %fusion.1), channel_id=1, replica_groups=mesh['pair'=1,'side'=2,'zh'=16,'zl'=2,'x'=4,'core'=2] {'zh'}, dimensions={0}, use_global_device_ids=true | all-gather | bytes 417792 | tf_op jit(solution)/shard_map/all_gather | solution.py:214
  69.8 4.0 %collective-permute-start.2 = (bf16[2,256,256]{2,1,0:T(8,128)(2,1)S(1)}, bf16[2,256,256]{2,1,0:T(8,128)(2,1)S(1)}, u32[]{:S(2)}, u32[]{:S(2)}) collective-permute-start(bf16[2,256,256]{2,1,0:T(8,128)(2,1)S(1)} %bitcast.31), channel_id=1, source_target_pairs={{0,256},{256,0},{1,257},{257,1},{2,258},{258,2},{3,259},{259,3},{4... | collective-permute-start | bytes 786440 | tf_op jit(solution)/shard_map/ppermute | solution.py:24
  73.8 3.7 %collective-permute-done.2 = bf16[2,256,256]{2,1,0:T(8,128)(2,1)S(1)} collective-permute-done((bf16[2,256,256]{2,1,0:T(8,128)(2,1)S(1)}, bf16[2,256,256]{2,1,0:T(8,128)(2,1)S(1)}, u32[]{:S(2)}, u32[]{:S(2)}) %collective-permute-start.2) | collective-permute-done | bytes 262176 | tf_op jit(solution)/shard_map/ppermute | solution.py:24
  77.6 3.4 %collective-permute-start.3 = (bf16[2,2,256,256]{3,2,1,0:T(8,128)(2,1)S(1)}, bf16[2,2,256,256]{3,2,1,0:T(8,128)(2,1)S(1)}, u32[]{:S(2)}, u32[]{:S(2)}) collective-permute-start(bf16[2,2,256,256]{3,2,1,0:T(8,128)(2,1)S(1)} %pad_maximum_fusion.1), channel_id=1, source_target_pairs={{0,8},{8,0},{1,9},{9,1},{2,10},{10,2},{3,11},{11,3},{4,12},{12,4},... | collective-permute-start | bytes 1572872 | tf_op jit(solution)/shard_map/ppermute | solution.py:24
  81.0 6.6 %collective-permute-done.3 = bf16[2,2,256,256]{3,2,1,0:T(8,128)(2,1)S(1)} collective-permute-done((bf16[2,2,256,256]{3,2,1,0:T(8,128)(2,1)S(1)}, bf16[2,2,256,256]{3,2,1,0:T(8,128)(2,1)S(1)}, u32[]{:S(2)}, u32[]{:S(2)}) %collective-permute-start.3) | collective-permute-done | bytes 524320 | tf_op jit(solution)/shard_map/ppermute | solution.py:24
  88.0 32.5 %all_to_all.10.w0_ref = bf16[4,3,2,256,256]{4,3,2,1,0:T(8,128)(2,1)} all-to-all(bf16[4,3,2,256,256]{4,3,2,1,0:T(8,128)(2,1)S(1)} %broadcast_in_dim.22), channel_id=1, replica_groups=mesh['pair'=1,'side'=2,'zh'=16,'zl'=2,'x'=4,'core'=2] {'x'}, dimensions={0} | all-to-all | bytes 6291456 | tf_op jit(solution)/shard_map/all_to_all | solution.py:20
  120.4 12.2 %collective-permute-start.4 = (bf16[4,3,2,256,256]{4,3,2,1,0:T(8,128)(2,1)}, bf16[4,3,2,256,256]{4,3,2,1,0:T(8,128)(2,1)}, u32[]{:S(2)}, u32[]{:S(2)}) collective-permute-start(bf16[4,3,2,256,256]{4,3,2,1,0:T(8,128)(2,1)} %all_to_all.10.w0_ref), channel_id=1, source_target_pairs={{0,1},{1,0},{2,3},{3,2},{4,5},{5,4},{6,7},{7,6},{8,9},{9,8},{10,11... | collective-permute-start | bytes 9437192 | tf_op jit(solution)/shard_map/ppermute | solution.py:24
  132.8 23.0 %all_to_all.11.w0_ref.refs_0_ = bf16[4,3,256,256]{3,2,1,0:T(8,128)(2,1)S(1)} all-to-all(bf16[4,3,256,256]{3,2,1,0:T(8,128)(2,1)S(1)} %broadcast_in_dim.20), channel_id=1, replica_groups=mesh['pair'=1,'side'=2,'zh'=16,'zl'=2,'x'=4,'core'=2] {'x'}, dimensions={0} | all-to-all | bytes 3145728 | tf_op jit(solution)/shard_map/all_to_all | solution.py:20
  155.8 3.1 %collective-permute-start.1 = (bf16[4,3,256,256]{3,2,1,0:T(8,128)(2,1)S(1)}, bf16[4,3,256,256]{3,2,1,0:T(8,128)(2,1)S(1)}, u32[]{:S(2)}, u32[]{:S(2)}) collective-permute-start(bf16[4,3,256,256]{3,2,1,0:T(8,128)(2,1)S(1)} %all_to_all.11.w0_ref.refs_0_), channel_id=1, source_target_pairs={{0,1},{1,0},{2,3},{3,2},{4,5},{5,4},{6,7},{7,6},{8,9},{9,8},{10,11... | collective-permute-start | bytes 4718600 | tf_op jit(solution)/shard_map/ppermute | solution.py:24
  158.9 3.4 %collective-permute-start.6 = (bf16[4,256,256]{2,1,0:T(8,128)(2,1)S(1)}, bf16[4,256,256]{2,1,0:T(8,128)(2,1)}, u32[]{:S(2)}, u32[]{:S(2)}) collective-permute-start(bf16[4,256,256]{2,1,0:T(8,128)(2,1)S(1)} %slice_bitcast_fusion), channel_id=1, source_target_pairs={{0,8},{8,0},{1,9},{9,1},{2,10},{10,2},{3,11},{11,3},{4,12},{12,4},... | collective-permute-start | bytes 1572872 | tf_op jit(solution)/shard_map/ppermute | solution.py:24
  162.3 3.4 %collective-permute-start.5 = (bf16[4,256,256]{2,1,0:T(8,128)(2,1)S(1)}, bf16[4,256,256]{2,1,0:T(8,128)(2,1)}, u32[]{:S(2)}, u32[]{:S(2)}) collective-permute-start(bf16[4,256,256]{2,1,0:T(8,128)(2,1)S(1)} %slice_bitcast_fusion), channel_id=1, source_target_pairs={{0,256},{256,0},{1,257},{257,1},{2,258},{258,2},{3,259},{259,3},{4... | collective-permute-start | bytes 1572872 | tf_op jit(solution)/shard_map/ppermute | solution.py:24
  165.7 8.7 %collective-permute-done.6.refs_2_ = bf16[4,256,256]{2,1,0:T(8,128)(2,1)} collective-permute-done((bf16[4,256,256]{2,1,0:T(8,128)(2,1)S(1)}, bf16[4,256,256]{2,1,0:T(8,128)(2,1)}, u32[]{:S(2)}, u32[]{:S(2)}) %collective-permute-start.6) | collective-permute-done | bytes 524320 | tf_op jit(solution)/shard_map/ppermute | solution.py:24
  174.4 3.4 %collective-permute-start.7 = (bf16[4,256,256]{2,1,0:T(8,128)(2,1)}, bf16[4,256,256]{2,1,0:T(8,128)(2,1)}, u32[]{:S(2)}, u32[]{:S(2)}) collective-permute-start(bf16[4,256,256]{2,1,0:T(8,128)(2,1)} %collective-permute-done.6.refs_2_), channel_id=1, source_target_pairs={{0,256},{256,0},{1,257},{257,1},{2,258},{258,2},{3,259},{259,3},{4... | collective-permute-start | bytes 1572872 | tf_op jit(solution)/shard_map/ppermute | solution.py:24
  177.8 0.9 slice_bitcast_fusion.1
  178.8 3.4 %collective-permute-start = (bf16[32,2048]{1,0:T(8,128)(2,1)S(1)}, bf16[32,2048]{1,0:T(8,128)(2,1)S(1)}, u32[]{:S(2)}, u32[]{:S(2)}) collective-permute-start(bf16[32,2048]{1,0:T(8,128)(2,1)S(1)} %slice_bitcast_fusion.1), channel_id=1, source_target_pairs={{0,8},{8,16},{16,24},{24,32},{32,40},{40,48},{48,56},{56,64},{64,7... | collective-permute-start | bytes 393224 | tf_op jit(solution)/shard_map/ppermute | solution.py:223
  182.2 1.9 collective-permute-done.halo_ref
  184.1 3.9 %collective-permute-start.9 = (bf16[4,256,256]{2,1,0:T(8,128)(2,1)}, bf16[4,256,256]{2,1,0:T(8,128)(2,1)}, u32[]{:S(2)}, u32[]{:S(2)}) collective-permute-start(bf16[4,256,256]{2,1,0:T(8,128)(2,1)} %collective-permute-done.6.refs_2_), channel_id=1, source_target_pairs={{0,1},{1,0},{2,3},{3,2},{4,5},{5,4},{6,7},{7,6},{8,9},{9,8},{10,11... | collective-permute-start | bytes 1572872 | tf_op jit(solution)/shard_map/ppermute | solution.py:24
  188.0 2.0 collective-permute-start.8
  190.0 3.1 %collective-permute-start.10 = (bf16[4,256,256]{2,1,0:T(8,128)(2,1)}, bf16[4,256,256]{2,1,0:T(8,128)(2,1)}, u32[]{:S(2)}, u32[]{:S(2)}) collective-permute-start(bf16[4,256,256]{2,1,0:T(8,128)(2,1)} %collective-permute-done.7.refs_3_), channel_id=1, source_target_pairs={{0,1},{1,0},{2,3},{3,2},{4,5},{5,4},{6,7},{7,6},{8,9},{9,8},{10,11... | collective-permute-start | bytes 1572872 | tf_op jit(solution)/shard_map/ppermute | solution.py:24
  193.1 0.6 pad_add_fusion.where_ref
  193.8 1.1 copy-done.1
  194.9 6.5 %shard_map.73 = (bf16[384,256]{1,0:T(8,128)(2,1)}, f32[2,384,128]{2,1,0:T(8,128)}, bf16[416,2048]{1,0:T(8,128)(2,1)}, f32[4,31,256]{2,1,0:T(8,128)}, f32[8,1024]{1,0:T(8,128)}) custom-call(s32[3]{0:T(128)} %pad_add_fusion.where_ref, bf16[32,2048]{1,0:T(8,128)(2,1)} %copy-done.2, bf16[384,2048]{1,0:T(8,128)(2,1)} %bitcast.29, bf16[31,1024]{1,0:T(8,128)(2,1)} %cw_ref.1, ...), custom_call_target="tpu_custom_call" | custom-call | flops 805306368 | bytes 8388608 | tf_op jit(solution)/shard_map/pallas_call | solution.py:192
  201.5 13.8 %shard_map.74 = bf16[384,2048]{1,0:T(8,128)(2,1)} custom-call(s32[3]{0:T(128)} %pad_add_fusion.where_ref, bf16[416,2048]{1,0:T(8,128)(2,1)} %get-tuple-element.10.tok_ref, f32[4,31,256]{2,1,0:T(8,128)} %get-tuple-element.11.cw_ref, f32[8,1024]{1,0:T(8,128)} %get-tuple-element.12.affine_ref, bf16[4,3,2,256,256]{4,3,2,1,0:T(8,128)(2,1)} %all_to_all.10.w0_ref, ...), custom_call_target="tpu_custom_call" | custom-call | flops 2415919104 | bytes 8388608 | tf_op jit(solution)/shard_map/pallas_call | solution.py:192
  (20 shorter events, 0.7 us)
Async XLA Ops:
  69.8 7.7 %collective-permute-start.2 = (bf16[2,256,256]{2,1,0:T(8,128)(2,1)S(1)}, bf16[2,256,256]{2,1,0:T(8,128)(2,1)S(1)}, u32[]{:S(2)}, u32[]{:S(2)}) collective-permute-start(bf16[2,256,256]{2,1,0:T(8,128)(2,1)S(1)} %bitcast.31), channel_id=1, source_target_pairs={{0,256},{256,0},{1,257},{257,1},{2,258},{258,2},{3,259},{259,3},{4... | collective-permute-start | bytes 786440 | tf_op jit(solution)/shard_map/ppermute | solution.py:24
  77.6 10.0 %collective-permute-start.3 = (bf16[2,2,256,256]{3,2,1,0:T(8,128)(2,1)S(1)}, bf16[2,2,256,256]{3,2,1,0:T(8,128)(2,1)S(1)}, u32[]{:S(2)}, u32[]{:S(2)}) collective-permute-start(bf16[2,2,256,256]{3,2,1,0:T(8,128)(2,1)S(1)} %pad_maximum_fusion.1), channel_id=1, source_target_pairs={{0,8},{8,0},{1,9},{9,1},{2,10},{10,2},{3,11},{11,3},{4,12},{12,4},... | collective-permute-start | bytes 1572872 | tf_op jit(solution)/shard_map/ppermute | solution.py:24
  120.4 81.0 %collective-permute-start.4 = (bf16[4,3,2,256,256]{4,3,2,1,0:T(8,128)(2,1)}, bf16[4,3,2,256,256]{4,3,2,1,0:T(8,128)(2,1)}, u32[]{:S(2)}, u32[]{:S(2)}) collective-permute-start(bf16[4,3,2,256,256]{4,3,2,1,0:T(8,128)(2,1)} %all_to_all.10.w0_ref), channel_id=1, source_target_pairs={{0,1},{1,0},{2,3},{3,2},{4,5},{5,4},{6,7},{7,6},{8,9},{9,8},{10,11... | collective-permute-start | bytes 9437192 | tf_op jit(solution)/shard_map/ppermute | solution.py:24
  155.8 38.0 %copy-start = (bf16[4,3,256,256]{3,2,1,0:T(8,128)(2,1)}, bf16[4,3,256,256]{3,2,1,0:T(8,128)(2,1)S(1)}, u32[]{:S(2)}) copy-start(bf16[4,3,256,256]{3,2,1,0:T(8,128)(2,1)S(1)} %all_to_all.11.w0_ref.refs_0_) | copy-start | bytes 4718596
  155.8 38.0 %collective-permute-start.1 = (bf16[4,3,256,256]{3,2,1,0:T(8,128)(2,1)S(1)}, bf16[4,3,256,256]{3,2,1,0:T(8,128)(2,1)S(1)}, u32[]{:S(2)}, u32[]{:S(2)}) collective-permute-start(bf16[4,3,256,256]{3,2,1,0:T(8,128)(2,1)S(1)} %all_to_all.11.w0_ref.refs_0_), channel_id=1, source_target_pairs={{0,1},{1,0},{2,3},{3,2},{4,5},{5,4},{6,7},{7,6},{8,9},{9,8},{10,11... | collective-permute-start | bytes 4718600 | tf_op jit(solution)/shard_map/ppermute | solution.py:24
  158.9 15.5 %collective-permute-start.6 = (bf16[4,256,256]{2,1,0:T(8,128)(2,1)S(1)}, bf16[4,256,256]{2,1,0:T(8,128)(2,1)}, u32[]{:S(2)}, u32[]{:S(2)}) collective-permute-start(bf16[4,256,256]{2,1,0:T(8,128)(2,1)S(1)} %slice_bitcast_fusion), channel_id=1, source_target_pairs={{0,8},{8,0},{1,9},{9,1},{2,10},{10,2},{3,11},{11,3},{4,12},{12,4},... | collective-permute-start | bytes 1572872 | tf_op jit(solution)/shard_map/ppermute | solution.py:24
  162.3 25.7 %collective-permute-start.5 = (bf16[4,256,256]{2,1,0:T(8,128)(2,1)S(1)}, bf16[4,256,256]{2,1,0:T(8,128)(2,1)}, u32[]{:S(2)}, u32[]{:S(2)}) collective-permute-start(bf16[4,256,256]{2,1,0:T(8,128)(2,1)S(1)} %slice_bitcast_fusion), channel_id=1, source_target_pairs={{0,256},{256,0},{1,257},{257,1},{2,258},{258,2},{3,259},{259,3},{4... | collective-permute-start | bytes 1572872 | tf_op jit(solution)/shard_map/ppermute | solution.py:24
  174.4 15.5 %collective-permute-start.7 = (bf16[4,256,256]{2,1,0:T(8,128)(2,1)}, bf16[4,256,256]{2,1,0:T(8,128)(2,1)}, u32[]{:S(2)}, u32[]{:S(2)}) collective-permute-start(bf16[4,256,256]{2,1,0:T(8,128)(2,1)} %collective-permute-done.6.refs_2_), channel_id=1, source_target_pairs={{0,256},{256,0},{1,257},{257,1},{2,258},{258,2},{3,259},{259,3},{4... | collective-permute-start | bytes 1572872 | tf_op jit(solution)/shard_map/ppermute | solution.py:24
  178.8 5.3 %collective-permute-start = (bf16[32,2048]{1,0:T(8,128)(2,1)S(1)}, bf16[32,2048]{1,0:T(8,128)(2,1)S(1)}, u32[]{:S(2)}, u32[]{:S(2)}) collective-permute-start(bf16[32,2048]{1,0:T(8,128)(2,1)S(1)} %slice_bitcast_fusion.1), channel_id=1, source_target_pairs={{0,8},{8,16},{16,24},{24,32},{32,40},{40,48},{48,56},{56,64},{64,7... | collective-permute-start | bytes 393224 | tf_op jit(solution)/shard_map/ppermute | solution.py:223
  184.1 9.7 %copy-start.2 = (bf16[32,2048]{1,0:T(8,128)(2,1)}, bf16[32,2048]{1,0:T(8,128)(2,1)S(1)}, u32[]{:S(2)}) copy-start(bf16[32,2048]{1,0:T(8,128)(2,1)S(1)} %collective-permute-done.halo_ref) | copy-start | bytes 393220
  184.1 17.3 %collective-permute-start.9 = (bf16[4,256,256]{2,1,0:T(8,128)(2,1)}, bf16[4,256,256]{2,1,0:T(8,128)(2,1)}, u32[]{:S(2)}, u32[]{:S(2)}) collective-permute-start(bf16[4,256,256]{2,1,0:T(8,128)(2,1)} %collective-permute-done.6.refs_2_), channel_id=1, source_target_pairs={{0,1},{1,0},{2,3},{3,2},{4,5},{5,4},{6,7},{7,6},{8,9},{9,8},{10,11... | collective-permute-start | bytes 1572872 | tf_op jit(solution)/shard_map/ppermute | solution.py:24
  188.0 13.4 %collective-permute-start.8 = (bf16[4,256,256]{2,1,0:T(8,128)(2,1)}, bf16[4,256,256]{2,1,0:T(8,128)(2,1)}, u32[]{:S(2)}, u32[]{:S(2)}) collective-permute-start(bf16[4,256,256]{2,1,0:T(8,128)(2,1)} %collective-permute-done.5.refs_1_), channel_id=1, source_target_pairs={{0,1},{1,0},{2,3},{3,2},{4,5},{5,4},{6,7},{7,6},{8,9},{9,8},{10,11... | collective-permute-start | bytes 1572872 | tf_op jit(solution)/shard_map/ppermute | solution.py:24
  190.0 11.4 %collective-permute-start.10 = (bf16[4,256,256]{2,1,0:T(8,128)(2,1)}, bf16[4,256,256]{2,1,0:T(8,128)(2,1)}, u32[]{:S(2)}, u32[]{:S(2)}) collective-permute-start(bf16[4,256,256]{2,1,0:T(8,128)(2,1)} %collective-permute-done.7.refs_3_), channel_id=1, source_target_pairs={{0,1},{1,0},{2,3},{3,2},{4,5},{5,4},{6,7},{7,6},{8,9},{9,8},{10,11... | collective-permute-start | bytes 1572872 | tf_op jit(solution)/shard_map/ppermute | solution.py:24
  193.8 1.1 copy-start.1
